TPU v7x, 256 devices: a whole 4x4x8 slice. The times are simulated.
256 devices in a mesh: sp: 16 (over y, x), tp: 16 (over z, core).
Axes of the slice: x: 4, y: 4, z: 8, core: 2. Of those that a mesh axis runs over, the one named last changes fastest.
Arguments:
- queries: bfloat16 [32768, 2048], P('sp', 'tp'), may hold values from -160 to 160
- key_heads: bfloat16 [32768, 512], P('sp'), may hold values from -8 to 8
- value_heads: bfloat16 [32768, 512], P('sp'), may hold values from -4 to 4
- sink_logit: float32 [16], P('tp'), may hold values from -2 to 7
- out_weight: bfloat16 [2048, 2048], P('tp'), may hold values from -0.125 to 0.125
- residual: bfloat16 [32768, 2048], P(('sp', 'tp')), may hold values from -6 to 6
- mixer_gain: float32 [2048], replicated, may hold values from 0.1 to 1.9
- expert_gain: float32 [2048], replicated, may hold values from 0.1 to 1.9
- route_group: int32 [32768], P(('sp', 'tp')), may hold values from 0 to 15, as said below
- route_member: int32 [32768, 2], P(('sp', 'tp')), may hold values from 0 to 2, as said below
- route_weight: bfloat16 [32768, 2], P(('sp', 'tp')), may hold values from 0.19921875 to 1
- gate_weight: bfloat16 [48, 2048, 2048], P('sp', None, 'tp'), may hold values from -0.125 to 0.125
- up_weight: bfloat16 [48, 2048, 2048], P('sp', None, 'tp'), may hold values from -0.125 to 0.125
- down_weight: bfloat16 [48, 2048, 2048], P('sp', 'tp'), may hold values from -0.125 to 0.125
Outputs:
- output: bfloat16 [32768, 2048], P(('sp', 'tp'))
Inputs may be any that keep to these rules, and one draw needn't show every extreme that they name: `route_group`: among the tokens of one device, at most 10 name one group; in every draw one group is named by exactly 10 tokens of every device. `route_member`: the two entries of a token are different members of its group.
All inputs are finite; a program needn't handle non-finite values.
Results may differ from a plain program's by a relative error of at most 0.018.
Values may be sent and summed in bfloat16 or wider, within the bound.
A program may use at most 128 MiB of HBM per device.

v0:
```python
import jax
import jax.numpy as jnp
from jax import lax
from jax.sharding import Mesh
from jax.sharding import PartitionSpec as P

HEADS = 16
KV_HEADS = 4
HEAD_DIM = 128
WINDOW = 128
BLOCK = 128
GROUP_EXPERTS = 3
TP = ("tp_0", "tp_1")
SP_TP = ("sp", "tp_0", "tp_1")


EPS = 1e-06
NEG_BIG = -1e30


def extended(block, sides, width):
    for axis, dim in sides:
        count = lax.axis_size(axis)
        forward = [(i, i + 1) for i in range(count - 1)]
        backward = [(target, source) for source, target in forward]
        low = lax.ppermute(
            lax.slice_in_dim(block, block.shape[dim] - width, None, axis=dim), axis, forward
        )
        high = lax.ppermute(lax.slice_in_dim(block, 0, width, axis=dim), axis, backward)
        block = jnp.concatenate([low, block, high], axis=dim)
    return block


def cut_along(shard, dim, devices):
    dims = shard.shape
    blocks = shard.reshape(*dims[:dim], devices, dims[dim] // devices, *dims[dim + 1 :])
    return jnp.moveaxis(blocks, dim, 0)


def joined_along(blocks, dim):
    dims = list(blocks.shape[1:])
    dims[dim] *= blocks.shape[0]
    return jnp.moveaxis(blocks, 0, dim).reshape(dims)


def exchange_in_order(blocks, axes, order):
    dims = [lax.axis_size(a) for a in axes]
    blocks = blocks.reshape(*dims, *blocks.shape[1:])
    for k in order:
        blocks = lax.all_to_all(blocks, axes[k], split_axis=k, concat_axis=k, tiled=True)
    return blocks.reshape(-1, *blocks.shape[len(axes) :])


def stepwise_exchange(shard, axes, order, split_dim, concat_dim):
    blocks = cut_along(shard, split_dim, lax.axis_size(axes))
    return joined_along(exchange_in_order(blocks, axes, order), concat_dim)


def window_attention(queries, key_heads, value_heads, sink_logit):
    seq_rows = queries.shape[0]
    heads_dev = sink_logit.shape[0]
    key_group = HEADS // KV_HEADS
    key_start = lax.axis_index(TP) * heads_dev // key_group * HEAD_DIM
    key_own = lax.dynamic_slice_in_dim(key_heads, key_start, HEAD_DIM, 1)
    value_own = lax.dynamic_slice_in_dim(value_heads, key_start, HEAD_DIM, 1)
    padded = extended(jnp.stack([key_own, value_own]), (("sp", 1),), WINDOW)
    blocks = seq_rows // BLOCK
    extent = WINDOW // BLOCK
    tile_rows = padded.reshape(2, blocks + 2 * extent, BLOCK, HEAD_DIM)
    key_spans = jnp.concatenate(
        [tile_rows[:, shifted : shifted + blocks] for shifted in range(2 * extent + 1)], axis=2
    )
    offset = lax.axis_index("sp") * seq_rows
    seq_total = seq_rows * lax.axis_size("sp")
    query_pos = offset + jnp.arange(seq_rows, dtype=jnp.int32).reshape(blocks, BLOCK)
    key_pos = (
        offset
        + (jnp.arange(blocks, dtype=jnp.int32) * BLOCK)[:, None]
        + jnp.arange(BLOCK + 2 * WINDOW, dtype=jnp.int32)[None, :]
        - WINDOW
    )
    inside = (
        (jnp.abs(query_pos[:, :, None] - key_pos[:, None, :]) <= WINDOW)
        & (key_pos >= 0)[:, None, :]
        & (key_pos < seq_total)[:, None, :]
    )
    query_blocks = queries.reshape(blocks, BLOCK, heads_dev, HEAD_DIM)
    scores = jnp.einsum(
        "nqhd,nkd->nhqk", query_blocks, key_spans[0], preferred_element_type=jnp.float32
    ) * HEAD_DIM ** (-0.5)
    scores = jnp.where(inside[:, None], scores, NEG_BIG)
    sink_col = sink_logit[None, :, None, None]
    row_top = jnp.maximum(jnp.max(scores, axis=3, keepdims=True), sink_col)
    exp_terms = jnp.exp(scores - row_top)
    row_mass = jnp.sum(exp_terms, axis=3, keepdims=True) + jnp.exp(sink_col - row_top)
    weight = (exp_terms / row_mass).astype(jnp.bfloat16)
    attended = jnp.einsum(
        "nhqk,nkd->nqhd", weight, key_spans[1], preferred_element_type=jnp.float32
    ).astype(jnp.bfloat16)
    return attended.reshape(seq_rows, heads_dev * HEAD_DIM)


def per_device(
    queries,
    key_heads,
    value_heads,
    sink_logit,
    out_weight,
    residual,
    mixer_gain,
    expert_gain,
    route_group,
    route_member,
    route_weight,
    gate_weight,
    up_weight,
    down_weight,
):
    attended = window_attention(queries, key_heads, value_heads, sink_logit)
    tok_rows = residual.shape[0]
    width = out_weight.shape[1]
    by_token = stepwise_exchange(attended, TP, (1, 0), 0, 1)
    shard_rows = out_weight.shape[0]
    weight_piece = lax.all_gather(out_weight, TP, axis=0, tiled=True)
    shards = weight_piece.shape[0] // shard_rows
    columns = by_token
    columns = columns.reshape(tok_rows, shards, shard_rows)
    weight_slabs = weight_piece.reshape(shards, shard_rows, width)
    products = jnp.einsum("rkc,kcd->krd", columns, weight_slabs, preferred_element_type=jnp.float32)
    rounded = lax.optimization_barrier(products.astype(jnp.bfloat16))
    projected = jnp.sum(rounded.astype(jnp.float32), axis=0)
    proj_scale = lax.rsqrt(jnp.mean(projected * projected, axis=1, keepdims=True) + EPS)
    mixed_rows = (residual.astype(jnp.float32) + mixer_gain * (projected * proj_scale)).astype(
        jnp.bfloat16
    )
    mixed_float = mixed_rows.astype(jnp.float32)
    norm_scale = lax.rsqrt(jnp.mean(mixed_float * mixed_float, axis=1, keepdims=True) + EPS)
    normed = (mixed_float * norm_scale * expert_gain).astype(jnp.bfloat16)
    groups = lax.axis_size("sp")
    capacity = max(2, (5 * tok_rows + 4 * groups - 1) // (4 * groups))
    group_ids = jnp.arange(groups, dtype=jnp.int32)
    chosen = (route_group[:, None] == group_ids[None, :]).astype(jnp.int32)
    group_rank = jnp.sum(chosen * (jnp.cumsum(chosen, axis=0) - 1), axis=1)
    slot_ids = route_group * capacity + group_rank
    placing = (jnp.arange(groups * capacity, dtype=jnp.int32)[:, None] == slot_ids[None, :]).astype(
        jnp.bfloat16
    )
    member_ids = jnp.arange(GROUP_EXPERTS, dtype=jnp.int32)
    token_gates = jnp.sum(
        route_weight.astype(jnp.float32)[:, :, None]
        * (route_member[:, :, None] == member_ids[None, None, :]).astype(jnp.float32),
        axis=1,
    ).astype(jnp.bfloat16)
    send_rows = (
        jnp.dot(placing, normed, preferred_element_type=jnp.float32)
        .astype(jnp.bfloat16)
        .reshape(groups, capacity, width)
    )
    send_gates = (
        jnp.dot(placing, token_gates, preferred_element_type=jnp.float32)
        .astype(jnp.bfloat16)
        .reshape(groups, capacity, GROUP_EXPERTS)
    )
    arrived_rows, arrived_gates = (
        lax.all_to_all(send_rows, "sp", split_axis=0, concat_axis=0, tiled=True),
        lax.all_to_all(send_gates, "sp", split_axis=0, concat_axis=0, tiled=True),
    )
    pooled_rows, pooled_gates = (
        lax.all_gather(arrived_rows, TP, axis=0, tiled=True),
        lax.all_gather(arrived_gates, TP, axis=0, tiled=True),
    )
    flat_rows = pooled_rows.reshape(-1, width)
    flat_gates = pooled_gates.reshape(-1, GROUP_EXPERTS).astype(jnp.float32)
    gate_pre = jnp.einsum("md,edh->meh", flat_rows, gate_weight, preferred_element_type=jnp.float32)
    up_pre = jnp.einsum("md,edh->meh", flat_rows, up_weight, preferred_element_type=jnp.float32)
    hidden = (jax.nn.silu(gate_pre) * up_pre * flat_gates[:, :, None]).astype(jnp.bfloat16)
    partial_out = jnp.einsum("meh,ehd->md", hidden, down_weight, preferred_element_type=jnp.float32)
    summed = lax.psum_scatter(
        partial_out.reshape(pooled_rows.shape).astype(jnp.bfloat16),
        TP,
        scatter_dimension=0,
        tiled=True,
    )
    returned = lax.all_to_all(summed, "sp", split_axis=0, concat_axis=0, tiled=True)
    expert_out = lax.dot_general(
        placing,
        returned.reshape(groups * capacity, width),
        (((0,), (0,)), ((), ())),
        preferred_element_type=jnp.float32,
    )
    return (mixed_float + expert_out).astype(jnp.bfloat16)


def solution(mesh):
    torus = Mesh(mesh.devices.reshape(mesh.shape["sp"], 8, 2), ("sp", "tp_0", "tp_1"))
    placed = (
        P("sp", TP),
        P("sp", None),
        P("sp", None),
        P(TP),
        P(TP, None),
        P(SP_TP, None),
        P(),
        P(),
        P(SP_TP),
        P(SP_TP, None),
        P(SP_TP, None),
        P("sp", None, TP),
        P("sp", None, TP),
        P("sp", TP, None),
    )
    return jax.shard_map(
        per_device, mesh=torus, in_specs=placed, out_specs=P(SP_TP, None), check_vma=False
    )
```

profile of v0, /device:TPU:8, one launch (start us, length us, event | category | flops | bytes accessed | tf_op | source)
XLA Modules:
  0.0 385.5 jit_solution(15848808001674454527)
XLA Ops:
  6.5 0.0 copy-start
  6.5 0.0 all-gather.3.cloned.1.call-start
  6.5 0.7 all-gather.3.cloned.1.call-update
  7.3 1.3 dynamic-slice_bitcast_fusion
  8.6 3.4 collective-permute-start
  12.0 4.6 %collective-permute-start.1 = (bf16[2,128,128]{2,1,0:T(8,128)(2,1)S(1)}, bf16[2,128,128]{2,1,0:T(8,128)(2,1)S(1)}, u32[]{:S(2)}, u32[]{:S(2)}) collective-permute-start(bf16[2,128,128]{2,1,0:T(8,128)(2,1)S(1)} %get-tuple-element.11), channel_id=1, source_target_pairs={{16,0},{32,16},{48,32},{64,48},{80,64},{96,80},{112,96},{128,112},... | collective-permute-start | bytes 196616 | tf_op jit(solution)/shard_map/ppermute | solution.py:29
  17.2 0.1 fusion.22
  17.3 0.1 add_add_fusion
  17.4 0.0 collective-permute-done
  17.4 1.0 collective-permute-done.1
  18.4 0.1 pad_maximum_fusion.1
  18.5 0.8 fusion.25
  19.3 0.0 copy-start.6
  19.3 0.4 pad_maximum_fusion
  19.7 0.6 copy-done.6
  20.4 4.1 %fusion.26 = (f32[16,128]{1,0:T(8,128)S(1)}, f32[16,1,128,384]{2,3,0,1:T(8,128)S(1)}) fusion(bf16[16,128,128]{2,1,0:T(8,128)(2,1)S(1)} %bitcast.66, bf16[2,16,384,128]{3,2,1,0:T(8,128)(2,1)S(1)} %pad_maximum_fusion, pred[16,384]{1,0:T(8,128)(4,1)S(1)} %get-tuple-element.13, pred[16,384]{1,0:T(8,128)(4,1)S(1)} %get-tuple-element.12, ...), kind=kOutput, calls=%fused_computation.58 | convolution fusion | flops 207616000 | bytes 5296128 | tf_op jit(solution)/shard_map/nqhd,nkd->nhqk/dot_general | solution.py:88
  24.5 0.4 fusion.4
  24.9 1.0 fusion.8
  26.0 0.0 copy-start.4
  26.1 4.2 %all_to_all.25 = bf16[8,2,128,128]{2,3,0,1:T(8,128)(2,1)S(1)} all-to-all(bf16[8,2,128,128]{2,3,0,1:T(8,128)(2,1)S(1)} %copy.57), channel_id=1, replica_groups=mesh['sp'=16,'tp_0'=8,'tp_1'=2] {'tp_1'}, dimensions={1} | all-to-all | bytes 1048576 | tf_op jit(solution)/shard_map/all_to_all | solution.py:50
  30.2 0.8 copy.58
  31.0 8.5 %all-to-all-start.1 = ((bf16[8,2,128,128]{2,3,1,0:T(8,128)(2,1)}), bf16[8,2,128,128]{2,3,1,0:T(8,128)(2,1)S(1)}, u32[]{:S(2)}, u32[]{:S(2)}) async-start(bf16[8,2,128,128]{2,3,1,0:T(8,128)(2,1)} %copy.58), calls=%async_computation.1 | async-start | bytes 1048576 | tf_op jit(solution)/shard_map/all_to_all | solution.py:50
  39.5 0.0 all-gather.5.cloned.1.call-start
  39.5 0.0 copy-done.4
  39.6 0.1 fusion.17
  39.6 0.2 reduce_window_sum.11
  39.8 0.2 select_reduce_fusion
  40.0 23.5 %all-to-all-done.1 = bf16[8,2,128,128]{2,3,1,0:T(8,128)(2,1)S(1)} async-done(((bf16[8,2,128,128]{2,3,1,0:T(8,128)(2,1)}), bf16[8,2,128,128]{2,3,1,0:T(8,128)(2,1)S(1)}, u32[]{:S(2)}, u32[]{:S(2)}) %all-to-all-start.1) | async-done | bytes 524320 | tf_op jit(solution)/shard_map/all_to_all | solution.py:50
  63.5 0.3 copy.59
  63.8 15.4 %all-gather.3.cloned.1.call-done = bf16[2048,2048]{1,0:T(8,128)(2,1)} async-done(((bf16[128,2048]{1,0:T(8,128)(2,1)}), bf16[2048,2048]{1,0:T(8,128)(2,1)}) %all-gather.3.cloned.1.call-update) | async-done | bytes 8388624 | tf_op jit(solution)/shard_map/all_gather | solution.py:124
  79.2 5.7 %convolution_convert_fusion = bf16[16,128,2048]{2,1,0:T(8,128)(2,1)S(1)} fusion(bf16[128,16,128]{2,0,1:T(8,128)(2,1)S(1)} %bitcast.64, bf16[16,128,2048]{2,1,0:T(8,128)(2,1)} %bitcast.62), kind=kOutput, calls=%fused_computation.2 | convolution fusion | flops 1077936128 | bytes 17301504 | tf_op jit(solution)/shard_map/rkc,kcd->krd/dot_general | solution.py:129
  84.9 0.0 copy-start.1
  84.9 0.0 copy-start.2
  84.9 1.8 convert_reduce_fusion
  86.8 0.0 copy-start.3
  86.8 0.2 multiply_reduce_fusion
  87.0 0.0 copy-done.1
  87.0 0.4 fusion.11
  87.4 0.1 copy-done.3
  87.5 1.3 convolution_convert_fusion.1
  88.8 1.3 reshape.189
  90.1 22.0 %all_to_all.26 = bf16[16,10,2048]{2,1,0:T(8,128)(2,1)S(1)} all-to-all(bf16[16,10,2048]{2,1,0:T(8,128)(2,1)S(1)} %reshape.189), channel_id=1, replica_groups=mesh['sp'=16,'tp_0'=8,'tp_1'=2] {'sp'}, dimensions={0} | all-to-all | bytes 1310720 | tf_op jit(solution)/shard_map/all_to_all | solution.py:165
  112.1 1.2 copy.60
  113.3 0.0 all-gather.5.cloned.1.call-update
  113.3 0.0 reduce-scatter.2.cloned.1.call-start
  113.4 0.0 copy-done.7
  113.5 0.1 convolution_convert_fusion.2
  113.6 0.1 reshape.191
  113.7 11.7 %all_to_all.27 = bf16[16,10,3]{1,2,0:T(4,128)(2,1)S(1)} all-to-all(bf16[16,10,3]{1,2,0:T(4,128)(2,1)S(1)} %copy.62), channel_id=1, replica_groups=mesh['sp'=16,'tp_0'=8,'tp_1'=2] {'sp'}, dimensions={0} | all-to-all | bytes 1920 | tf_op jit(solution)/shard_map/all_to_all | solution.py:166
  125.4 18.3 %all_gather.11 = bf16[256,10,3]{1,2,0:T(4,128)(2,1)S(1)} all-gather(bf16[16,10,3]{1,2,0:T(4,128)(2,1)S(1)} %all_to_all.27), channel_id=1, replica_groups=mesh['sp'=16,'tp_0'=8,'tp_1'=2] {'tp_0','tp_1'}, dimensions={0}, use_global_device_ids=true | all-gather | bytes 16320 | tf_op jit(solution)/shard_map/all_gather | solution.py:170
  143.7 0.2 copy.63
  143.8 0.2 copy.64
  144.0 0.3 reshape.193
  144.3 33.3 %all-gather.5.cloned.1.call-done = bf16[256,10,2048]{2,0,1:T(8,128)(2,1)} async-done(((bf16[16,10,2048]{2,0,1:T(8,128)(2,1)}), bf16[256,10,2048]{2,0,1:T(8,128)(2,1)}) %all-gather.5.cloned.1.call-update) | async-done | bytes 10485776 | tf_op jit(solution)/shard_map/all_gather | solution.py:169
  177.6 15.4 %copy.61 = bf16[256,10,2048]{2,1,0:T(8,128)(2,1)} copy(bf16[256,10,2048]{2,0,1:T(8,128)(2,1)} %all-gather.5.cloned.1.call-done) | data formatting | bytes 20971520 | tf_op jit(solution)/shard_map/all_gather | solution.py:169
  193.0 18.1 %reshape.194 = bf16[2560,2048,1]{1,0,2:T(8,128)(2,1)} reshape(bf16[256,10,2048]{2,1,0:T(8,128)(2,1)} %copy.61) | data formatting | bytes 20971520 | tf_op jit(solution)/shard_map/reshape | solution.py:172
  211.1 10.0 %fusion.27 = f32[2560,3,128]{2,0,1:T(8,128)} fusion(bf16[2560,2048,1]{1,0,2:T(8,128)(2,1)} %reshape.194, bf16[3,2048,128]{2,1,0:T(8,128)(2,1)} %param.25), kind=kOutput, calls=%fused_computation.59 | convolution fusion | flops 4026531840 | bytes 15990784 | tf_op jit(solution)/shard_map/md,edh->meh/dot_general | solution.py:174
  221.1 16.4 %bitcast_convert_fusion = bf16[2560,2048]{1,0:T(8,128)(2,1)} fusion(bf16[3,128,2048]{2,1,0:T(8,128)(2,1)S(1)} %copy-done, bf16[2560,2048,1]{1,0,2:T(8,128)(2,1)} %reshape.194, bf16[3,2048,128]{2,1,0:T(8,128)(2,1)} %param.26, f32[2560,3,128]{2,0,1:T(8,128)} %fusion.27, f32[2560,3]{0,1:T(4,128)S(1)} %reshape.193), kind=kOutput, calls=%fused_computation | convolution fusion | flops 8065187840 | bytes 28080128 | tf_op jit(solution)/shard_map/meh,ehd->md/dot_general | solution.py:177
  237.5 17.7 %convert_element_type.88 = bf16[256,10,2048]{2,1,0:T(8,128)(2,1)} reshape(bf16[2560,2048]{1,0:T(8,128)(2,1)} %bitcast_convert_fusion) | data formatting | bytes 20971520 | tf_op jit(solution)/shard_map/convert_element_type | solution.py:179
  255.1 0.0 reduce-scatter.2.cloned.1.call-update
  255.2 99.2 %reduce-scatter.2.cloned.1.call-done = bf16[16,10,2048]{2,1,0:T(8,128)(2,1)} async-done(((bf16[256,10,2048]{2,1,0:T(8,128)(2,1)}), bf16[16,10,2048]{2,1,0:T(8,128)(2,1)}) %reduce-scatter.2.cloned.1.call-update) | async-done | bytes 655376 | tf_op jit(solution)/shard_map/reduce_scatter | solution.py:178
  354.4 21.2 %all_to_all.28 = bf16[16,10,2048]{2,1,0:T(8,128)(2,1)S(1)} all-to-all(bf16[16,10,2048]{2,1,0:T(8,128)(2,1)} %reduce-scatter.2.cloned.1.call-done), channel_id=1, replica_groups=mesh['sp'=16,'tp_0'=8,'tp_1'=2] {'sp'}, dimensions={0} | all-to-all | bytes 1310720 | tf_op jit(solution)/shard_map/all_to_all | solution.py:184
  375.6 1.1 reshape.192
  376.7 2.2 fusion.5
  (17 shorter events, 0.1 us)
Async XLA Ops:
  6.5 214.5 %copy-start = (bf16[3,128,2048]{2,1,0:T(8,128)(2,1)S(1)}, bf16[3,128,2048]{2,1,0:T(8,128)(2,1)}, u32[]{:S(2)}) copy-start(bf16[3,128,2048]{2,1,0:T(8,128)(2,1)} %param.27) | copy-start | bytes 4718596
  6.5 72.7 %all-gather.3.cloned.1.call-start = ((), (), s32[]{:S(2)}) async-start(), calls=%async_computation.6 | async-start | bytes 8912896 | tf_op jit(solution)/shard_map/all_gather | solution.py:124
  8.6 8.8 %collective-permute-start = (bf16[2,128,128]{2,1,0:T(8,128)(2,1)S(1)}, bf16[2,128,128]{2,1,0:T(8,128)(2,1)S(1)}, u32[]{:S(2)}, u32[]{:S(2)}) collective-permute-start(bf16[2,128,128]{2,1,0:T(8,128)(2,1)S(1)} %get-tuple-element.10), channel_id=1, source_target_pairs={{0,16},{16,32},{32,48},{48,64},{64,80},{80,96},{96,112},{112,128},... | collective-permute-start | bytes 196616 | tf_op jit(solution)/shard_map/ppermute | solution.py:26
  12.0 6.4 %collective-permute-start.1 = (bf16[2,128,128]{2,1,0:T(8,128)(2,1)S(1)}, bf16[2,128,128]{2,1,0:T(8,128)(2,1)S(1)}, u32[]{:S(2)}, u32[]{:S(2)}) collective-permute-start(bf16[2,128,128]{2,1,0:T(8,128)(2,1)S(1)} %get-tuple-element.11), channel_id=1, source_target_pairs={{16,0},{32,16},{48,32},{64,48},{80,64},{96,80},{112,96},{128,112},... | collective-permute-start | bytes 196616 | tf_op jit(solution)/shard_map/ppermute | solution.py:29
  19.3 1.0 copy-start.6
  26.0 13.6 %copy-start.4 = (s32[128]{0:T(128)S(1)}, s32[128]{0:T(128)}, u32[]{:S(2)}) copy-start(s32[128]{0:T(128)} %param.22) | copy-start | bytes 1540
  31.0 32.4 %all-to-all-start.1 = ((bf16[8,2,128,128]{2,3,1,0:T(8,128)(2,1)}), bf16[8,2,128,128]{2,3,1,0:T(8,128)(2,1)S(1)}, u32[]{:S(2)}, u32[]{:S(2)}) async-start(bf16[8,2,128,128]{2,3,1,0:T(8,128)(2,1)} %copy.58), calls=%async_computation.1 | async-start | bytes 1048576 | tf_op jit(solution)/shard_map/all_to_all | solution.py:50
  39.5 138.1 %all-gather.5.cloned.1.call-start = ((), (), s32[]{:S(2)}) async-start(), calls=%async_computation.7 | async-start | bytes 11141120 | tf_op jit(solution)/shard_map/all_gather | solution.py:169
  84.9 2.1 copy-start.1
  84.9 2.0 copy-start.2
  86.8 0.7 copy-start.3
  88.7 24.7 %copy-start.7 = (bf16[128,2]{0,1:T(2,128)(2,1)S(1)}, bf16[128,2]{0,1:T(2,128)(2,1)}, u32[]{:S(2)}) copy-start(bf16[128,2]{0,1:T(2,128)(2,1)} %param.24) | copy-start | bytes 1540
  88.8 24.7 %copy-start.5 = (s32[128,2]{0,1:T(2,128)S(1)}, s32[128,2]{0,1:T(2,128)}, u32[]{:S(2)}) copy-start(s32[128,2]{0,1:T(2,128)} %param.23) | copy-start | bytes 3076
  113.3 241.1 %reduce-scatter.2.cloned.1.call-start = ((), (), s32[]{:S(2)}) async-start(), calls=%async_computation.8 | async-start | bytes 17825792 | tf_op jit(solution)/shard_map/reduce_scatter | solution.py:178
Sparse Core Ops, SparseCore 0:
  9.2 69.9 all-gather.2
  113.5 64.0 all-gather.4
  255.3 99.0 reduce-scatter.1
where the time goes:
time: 389 us; the launch traced here: 385 us
  waiting for transfers between devices  173 us (44%)
  blocking collectives  77.4 us (20%)
  local copies, waits for them, and re-layouts  59.5 us (15%)
  matrix products  40.9 us (11%)
  starting transfers between devices  16.5 us (4%)
  between operations  14.1 us (4%)
  other arithmetic  3.92 us (1%)
    reduce_scatter x1, waiting for transfers between devices, per_device(): lax.psum_scatter(partial_out.reshape(pooled_rows.shape).astype(jnp.bfloat...  99.2 us
    all_gather x1, waiting for transfers between devices, per_device(): lax.all_gather(arrived_rows, TP, axis=0, tiled=True)  33.3 us
    all_to_all x1, waiting for transfers between devices, exchange_in_order(): lax.all_to_all(blocks, axes[k], split_axis=k, concat_axis=k, tiled=True)  23.5 us
    all_to_all x1, blocking collectives, per_device(): lax.all_to_all(send_rows, 'sp', split_axis=0, concat_axis=0, tiled=True)  22 us
    all_to_all x1, blocking collectives, per_device(): lax.all_to_all(summed, 'sp', split_axis=0, concat_axis=0, tiled=True)  21.2 us
    all_gather x1, blocking collectives, per_device(): lax.all_gather(arrived_gates, TP, axis=0, tiled=True)  18.3 us
    reshape x1, local copies, waits for them, and re-layouts, per_device(): flat_rows = pooled_rows.reshape(-1, width)  18.1 us
    convert_element_type x1, local copies, waits for them, and re-layouts, per_device(): partial_out.reshape(pooled_rows.shape).astype(jnp.bfloat16)  17.7 us
  transfers between devices with their start and end apart: 6, of which 5 were waited for; matrix products, arithmetic and copies ran while one was open for 3% of the time, Pallas kernels for 0%

commit v1 on v0

--- a/solution.py
+++ b/solution.py
@@ -1,6 +1,10 @@
+import functools
+
 import jax
 import jax.numpy as jnp
 from jax import lax
+from jax.experimental import pallas as pl
+from jax.experimental.pallas import tpu as pltpu
 from jax.sharding import Mesh
 from jax.sharding import PartitionSpec as P
 
@@ -16,6 +20,7 @@
 
 EPS = 1e-06
 NEG_BIG = -1e30
+VMEM_LIMIT = 60 * 1024 * 1024
 
 
 def extended(block, sides, width):
@@ -98,6 +103,366 @@
         "nhqk,nkd->nqhd", weight, key_spans[1], preferred_element_type=jnp.float32
     ).astype(jnp.bfloat16)
     return attended.reshape(seq_rows, heads_dev * HEAD_DIM)
+
+
+MESH_ID = pl.DeviceIdType.MESH
+SLOT = 16
+
+
+def expert_kernel(
+    n_sp,
+    n_z,
+    cap,
+    normed,
+    mixed,
+    placing,
+    placing_t,
+    gate_rows,
+    pick,
+    pick_t,
+    gate_pick,
+    wg,
+    wu,
+    wd,
+    out,
+    send,
+    arr,
+    rows,
+    gates,
+    gcol,
+    hidden,
+    w_in,
+    w_out,
+    own,
+    oth,
+    got,
+    hop,
+    ret,
+    back,
+    w_sem,
+    disp_s,
+    disp_r,
+    ring_s,
+    ring_r,
+    rgate_s,
+    rgate_r,
+    pair_s,
+    pair_r,
+    pgate_s,
+    pgate_r,
+    sum_s,
+    sum_r,
+    hop_s,
+    hop_r,
+    ret_s,
+    ret_r,
+):
+    sp, z, c = lax.axis_index("sp"), lax.axis_index("tp_0"), lax.axis_index("tp_1")
+    width = normed.shape[1]
+    experts, hid = wd.shape[0], wd.shape[1]
+    half = n_sp // 2
+    hr = half * cap
+    far = n_z // 2
+    tile = 256 if width % 256 == 0 else width
+    sends = []
+
+    def push(src, dst, s_sem, r_sem, dev):
+        copy = pltpu.make_async_remote_copy(
+            src_ref=src, dst_ref=dst, send_sem=s_sem, recv_sem=r_sem, device_id=dev, device_id_type=MESH_ID
+        )
+        copy.start()
+        sends.append(copy)
+        return copy
+
+    partner = (sp, z, 1 - c)
+    ring_dev = ((sp, lax.rem(z + 1, n_z), c), (sp, lax.rem(z + n_z - 1, n_z), c))
+
+    loads = []
+    for e in range(experts):
+        loads.append(pltpu.make_async_copy(wg.at[e], w_in.at[e, :, pl.ds(0, hid)], w_sem.at[e, 0]))
+        loads.append(pltpu.make_async_copy(wu.at[e], w_in.at[e, :, pl.ds(hid, hid)], w_sem.at[e, 1]))
+        loads.append(pltpu.make_async_copy(wd.at[e], w_out.at[pl.ds(e * hid, hid), :], w_sem.at[e, 2]))
+    for load in loads:
+        load.start()
+
+    barrier = pltpu.get_barrier_semaphore()
+    for j in range(1, n_sp):
+        pl.semaphore_signal(barrier, inc=1, device_id=(lax.rem(sp + j, n_sp), z, c), device_id_type=MESH_ID)
+    for dev in ring_dev + (partner,):
+        pl.semaphore_signal(barrier, inc=1, device_id=dev, device_id_type=MESH_ID)
+
+    head = jnp.dot(placing[...], normed[:, 0:128], preferred_element_type=jnp.float32)
+    send[:, 0:128] = (head + gate_rows[...].astype(jnp.float32)).astype(jnp.bfloat16)
+    send[:, 128:] = jnp.dot(placing[...], normed[:, 128:], preferred_element_type=jnp.float32).astype(
+        jnp.bfloat16
+    )
+    pl.semaphore_wait(barrier, n_sp - 1 + 3)
+
+    disp = [None]
+    for j in range(1, n_sp):
+        block = pl.ds(j * SLOT, SLOT)
+        disp.append(
+            push(send.at[block], arr.at[block], disp_s.at[j], disp_r.at[j], (lax.rem(sp + j, n_sp), z, c))
+        )
+    arr[0:SLOT] = send[0:SLOT]
+
+    def reach(dr, hf):
+        return far if dr == hf else far - 1
+
+    def at(dr, d):
+        return (n_z - d) % n_z if dr == 0 else d
+
+    def part(rc, hf):
+        return pl.ds((rc * 2 + hf) * hr, hr)
+
+    ring = {}
+    ring_g = {}
+    pair = {}
+
+    def ring_send(dr, d, hf):
+        src, dst = at(dr, d), at(dr, d + 1)
+        sem = (dr, d, hf)
+        ring[sem] = push(
+            rows.at[src, part(0, hf)], rows.at[dst, part(0, hf)], ring_s.at[sem], ring_r.at[sem], ring_dev[dr]
+        )
+        ring_g[sem] = push(
+            gates.at[src, 0, hf], gates.at[dst, 0, hf], rgate_s.at[sem], rgate_r.at[sem], ring_dev[dr]
+        )
+
+    def ring_wait(dr, d, hf):
+        ring[(dr, d - 1, hf)].wait_recv()
+        ring_g[(dr, d - 1, hf)].wait_recv()
+
+    def pair_send(o, hf):
+        pair[(o, hf)] = (
+            push(rows.at[o, part(0, hf)], rows.at[o, part(1, hf)], pair_s.at[o, hf], pair_r.at[o, hf], partner),
+            push(gates.at[o, 0, hf], gates.at[o, 1, hf], pgate_s.at[o, hf], pgate_r.at[o, hf], partner),
+        )
+
+    for hf in range(2):
+        for j in range(hf * half, (hf + 1) * half):
+            if j > 0:
+                disp[j].wait_recv()
+        block = pl.ds(hf * half * SLOT, half * SLOT)
+        rows[0, part(0, hf)] = jnp.dot(pick[...], arr[block, :], preferred_element_type=jnp.float32).astype(
+            jnp.bfloat16
+        )
+        gates[0, 0, hf] = jnp.dot(
+            gate_pick[...], arr[block, 0:128], preferred_element_type=jnp.float32
+        ).astype(jnp.bfloat16)
+        ring_send(0, 0, hf)
+        ring_send(1, 0, hf)
+        pair_send(0, hf)
+
+    for load in loads:
+        load.wait()
+
+    eye = jnp.where(
+        lax.broadcasted_iota(jnp.int32, (hr, 128), 0) == lax.broadcasted_iota(jnp.int32, (hr, 128), 1), 1.0, 0.0
+    ).astype(jnp.bfloat16)
+    summed = {}
+
+    def compute(o):
+        for hf in range(2):
+            for copy in pair[(o, hf)]:
+                copy.wait_recv()
+        for rc in range(2):
+            for hf in range(2):
+                gcol[part(rc, hf)] = lax.dot_general(
+                    eye, gates[o, rc, hf], (((1,), (1,)), ((), ())), preferred_element_type=jnp.float32
+                )
+        for e in range(experts):
+            pre = jnp.dot(rows[o], w_in[e], preferred_element_type=jnp.float32)
+            gate_pre, up_pre = pre[:, :hid], pre[:, hid:]
+            scaled = gate_pre / (1.0 + jnp.exp(-gate_pre)) * up_pre * gcol[:, e : e + 1]
+            hidden[:, e * hid : (e + 1) * hid] = scaled.astype(jnp.bfloat16)
+
+        def down(i, carry):
+            columns = pl.ds(pl.multiple_of(i * tile, tile), tile)
+            piece = jnp.dot(hidden[...], w_out[:, columns], preferred_element_type=jnp.float32).astype(
+                jnp.bfloat16
+            )
+            own[o, :, columns] = piece[: 2 * hr]
+            oth[o, :, columns] = piece[2 * hr :]
+            return carry
+
+        lax.fori_loop(0, width // tile, down, 0)
+        summed[o] = push(oth.at[o], got.at[o], sum_s.at[o], sum_r.at[o], partner)
+
+    hops = {}
+    settled = set()
+
+    def settle(o):
+        if o not in settled:
+            summed[o].wait_recv()
+            settled.add(o)
+
+    def half_rows(hf, i):
+        return pl.ds(pl.multiple_of(hf * hr + i * 16, 16), 16)
+
+    def hop_send(dr, d, hf):
+        o = (n_z - d) % n_z if dr == 1 else d
+        settle(o)
+        start = d == reach(dr, hf)
+        if start:
+            src = own.at[o, pl.ds(hf * hr, hr)]
+        else:
+            hops[(dr, d + 1, hf)].wait_recv()
+            src = hop.at[dr, d, hf]
+
+        def add(i, carry):
+            local = pl.ds(pl.multiple_of(i * 16, 16), 16)
+            total = own[o, half_rows(hf, i)].astype(jnp.float32) + got[o, half_rows(hf, i)].astype(jnp.float32)
+            if not start:
+                total = total + hop[dr, d, hf, local].astype(jnp.float32)
+            src[local] = total.astype(jnp.bfloat16)
+            return carry
+
+        lax.fori_loop(0, hr // 16, add, 0)
+        sem = (dr, d, hf)
+        hops[sem] = push(src, hop.at[dr, d - 1, hf], hop_s.at[sem], hop_r.at[sem], ring_dev[dr])
+
+    compute(0)
+    order = []
+    for d in range(1, far):
+        order += [(d, 0), (d, 1)]
+    for d, sub in order:
+        for dr in range(2):
+            hf = sub
+            ring_wait(dr, d, hf)
+            if d < reach(dr, hf):
+                ring_send(dr, d, hf)
+            pair_send(at(dr, d), hf)
+        if sub == 1:
+            compute(at(0, d))
+            compute(at(1, d))
+    for dr in range(2):
+        hop_send(dr, far - 1, 1 - dr)
+    for dr in range(2):
+        ring_wait(dr, far, dr)
+        pair_send(at(dr, far), dr)
+    compute(far)
+    for dr in range(2):
+        hop_send(dr, far, dr)
+    for d in range(far - 2, 0, -1):
+        for dr in range(2):
+            hop_send(dr, d, 1 - dr)
+        for dr in range(2):
+            hop_send(dr, d + 1, dr)
+    for dr in range(2):
+        hop_send(dr, 1, dr)
+
+    settle(0)
+    returned = [None] * n_sp
+    for hf in range(2):
+        for dr in range(2):
+            hops[(dr, 1, hf)].wait_recv()
+
+        def finish(i, carry):
+            local = pl.ds(pl.multiple_of(i * 16, 16), 16)
+            total = own[0, half_rows(hf, i)].astype(jnp.float32) + got[0, half_rows(hf, i)].astype(jnp.float32)
+            total = total + (hop[0, 0, hf, local].astype(jnp.float32) + hop[1, 0, hf, local].astype(jnp.float32))
+            own[0, half_rows(hf, i)] = total.astype(jnp.bfloat16)
+            return carry
+
+        lax.fori_loop(0, hr // 16, finish, 0)
+        ret[pl.ds(hf * half * SLOT, half * SLOT)] = jnp.dot(
+            pick_t[...], own[0, pl.ds(hf * hr, hr)], preferred_element_type=jnp.float32
+        ).astype(jnp.bfloat16)
+        for j in range(hf * half, (hf + 1) * half):
+            block = pl.ds(j * SLOT, SLOT)
+            if j == 0:
+                back[block] = ret[block]
+            else:
+                returned[j] = push(
+                    ret.at[block], back.at[block], ret_s.at[j], ret_r.at[j], (lax.rem(sp + n_sp - j, n_sp), z, c)
+                )
+    for j in range(1, n_sp):
+        returned[j].wait_recv()
+    expert_out = jnp.dot(placing_t[...], back[...], preferred_element_type=jnp.float32)
+    out[...] = (mixed[...].astype(jnp.float32) + expert_out).astype(jnp.bfloat16)
+    for copy in sends:
+        copy.wait_send()
+
+
+def routed_experts(normed, mixed, route_group, token_gates, wg, wu, wd, cap):
+    n_sp, n_z = lax.axis_size("sp"), lax.axis_size("tp_0")
+    tok_rows, width = normed.shape
+    experts, hid = wd.shape[0], wd.shape[1]
+    half = n_sp // 2
+    hr = half * cap
+    far = n_z // 2
+    group_ids = jnp.arange(n_sp, dtype=jnp.int32)
+    chosen = (route_group[:, None] == group_ids[None, :]).astype(jnp.int32)
+    rank = jnp.sum(chosen * (jnp.cumsum(chosen, axis=0) - 1), axis=1)
+    ahead = jnp.mod(route_group - lax.axis_index("sp"), n_sp)
+    slot = ahead * SLOT + rank
+    slots = jnp.arange(n_sp * SLOT, dtype=jnp.int32)
+    placing = (slots[:, None] == slot[None, :]).astype(jnp.bfloat16)
+    placing_t = (slot[:, None] == slots[None, :]).astype(jnp.bfloat16)
+    lane = jnp.mod(ahead, half) * cap + rank
+    lane_hot = (lane[:, None] == jnp.arange(128, dtype=jnp.int32)[None, :]).astype(jnp.float32)
+    members = jnp.arange(experts, dtype=jnp.int32)
+    row_at = (ahead * SLOT + cap)[None, :] + members[:, None]
+    row_hot = (slots[:, None, None] == row_at[None]).astype(jnp.bfloat16).reshape(n_sp * SLOT, -1)
+    lane_val = (token_gates.astype(jnp.float32).T[:, :, None] * lane_hot[None]).astype(jnp.bfloat16)
+    gate_rows = jnp.dot(row_hot, lane_val.reshape(-1, 128), preferred_element_type=jnp.float32).astype(
+        jnp.bfloat16
+    )
+    r = jnp.arange(hr, dtype=jnp.int32)
+    padded = r // cap * SLOT + r % cap
+    i = jnp.arange(half * SLOT, dtype=jnp.int32)
+    pick = (i[None, :] == padded[:, None]).astype(jnp.bfloat16)
+    pick_t = (i[:, None] == padded[None, :]).astype(jnp.bfloat16)
+    gate_pick = (
+        (i[None, :] % SLOT == jnp.arange(16, dtype=jnp.int32)[:, None] + cap) & (jnp.arange(16)[:, None] < experts)
+    ).astype(jnp.bfloat16)
+    bf = jnp.bfloat16
+    vmem = pl.BlockSpec(memory_space=pltpu.VMEM)
+    anywhere = pl.BlockSpec(memory_space=pl.ANY)
+    dma = pltpu.SemaphoreType.DMA
+    return pl.pallas_call(
+        functools.partial(expert_kernel, n_sp, n_z, cap),
+        out_shape=jax.ShapeDtypeStruct((tok_rows, width), bf),
+        in_specs=[vmem] * 8 + [anywhere] * 3,
+        out_specs=vmem,
+        scratch_shapes=[
+            pltpu.VMEM((n_sp * SLOT, width), bf),
+            pltpu.VMEM((n_sp * SLOT, width), bf),
+            pltpu.VMEM((n_z, 4 * hr, width), bf),
+            pltpu.VMEM((n_z, 2, 2, 16, 128), bf),
+            pltpu.VMEM((4 * hr, 16), jnp.float32),
+            pltpu.VMEM((4 * hr, experts * hid), bf),
+            pltpu.VMEM((experts, width, 2 * hid), bf),
+            pltpu.VMEM((experts * hid, width), bf),
+            pltpu.VMEM((n_z, 2 * hr, width), bf),
+            pltpu.VMEM((n_z, 2 * hr, width), bf),
+            pltpu.VMEM((n_z, 2 * hr, width), bf),
+            pltpu.VMEM((2, far, 2, hr, width), bf),
+            pltpu.VMEM((n_sp * SLOT, width), bf),
+            pltpu.VMEM((n_sp * SLOT, width), bf),
+            dma((experts, 3)),
+            dma((n_sp,)),
+            dma((n_sp,)),
+            dma((2, far, 2)),
+            dma((2, far, 2)),
+            dma((2, far, 2)),
+            dma((2, far, 2)),
+            dma((n_z, 2)),
+            dma((n_z, 2)),
+            dma((n_z, 2)),
+            dma((n_z, 2)),
+            dma((n_z,)),
+            dma((n_z,)),
+            dma((2, far + 1, 2)),
+            dma((2, far + 1, 2)),
+            dma((n_sp,)),
+            dma((n_sp,)),
+        ],
+        compiler_params=pltpu.CompilerParams(
+            collective_id=1, has_side_effects=True, vmem_limit_bytes=VMEM_LIMIT
+        ),
+    )(normed, mixed, placing, placing_t, gate_rows, pick, pick_t, gate_pick, wg, wu, wd)
 
 
 def per_device(
@@ -138,57 +503,15 @@
     normed = (mixed_float * norm_scale * expert_gain).astype(jnp.bfloat16)
     groups = lax.axis_size("sp")
     capacity = max(2, (5 * tok_rows + 4 * groups - 1) // (4 * groups))
-    group_ids = jnp.arange(groups, dtype=jnp.int32)
-    chosen = (route_group[:, None] == group_ids[None, :]).astype(jnp.int32)
-    group_rank = jnp.sum(chosen * (jnp.cumsum(chosen, axis=0) - 1), axis=1)
-    slot_ids = route_group * capacity + group_rank
-    placing = (jnp.arange(groups * capacity, dtype=jnp.int32)[:, None] == slot_ids[None, :]).astype(
-        jnp.bfloat16
-    )
     member_ids = jnp.arange(GROUP_EXPERTS, dtype=jnp.int32)
     token_gates = jnp.sum(
         route_weight.astype(jnp.float32)[:, :, None]
         * (route_member[:, :, None] == member_ids[None, None, :]).astype(jnp.float32),
         axis=1,
-    ).astype(jnp.bfloat16)
-    send_rows = (
-        jnp.dot(placing, normed, preferred_element_type=jnp.float32)
-        .astype(jnp.bfloat16)
-        .reshape(groups, capacity, width)
-    )
-    send_gates = (
-        jnp.dot(placing, token_gates, preferred_element_type=jnp.float32)
-        .astype(jnp.bfloat16)
-        .reshape(groups, capacity, GROUP_EXPERTS)
-    )
-    arrived_rows, arrived_gates = (
-        lax.all_to_all(send_rows, "sp", split_axis=0, concat_axis=0, tiled=True),
-        lax.all_to_all(send_gates, "sp", split_axis=0, concat_axis=0, tiled=True),
-    )
-    pooled_rows, pooled_gates = (
-        lax.all_gather(arrived_rows, TP, axis=0, tiled=True),
-        lax.all_gather(arrived_gates, TP, axis=0, tiled=True),
-    )
-    flat_rows = pooled_rows.reshape(-1, width)
-    flat_gates = pooled_gates.reshape(-1, GROUP_EXPERTS).astype(jnp.float32)
-    gate_pre = jnp.einsum("md,edh->meh", flat_rows, gate_weight, preferred_element_type=jnp.float32)
-    up_pre = jnp.einsum("md,edh->meh", flat_rows, up_weight, preferred_element_type=jnp.float32)
-    hidden = (jax.nn.silu(gate_pre) * up_pre * flat_gates[:, :, None]).astype(jnp.bfloat16)
-    partial_out = jnp.einsum("meh,ehd->md", hidden, down_weight, preferred_element_type=jnp.float32)
-    summed = lax.psum_scatter(
-        partial_out.reshape(pooled_rows.shape).astype(jnp.bfloat16),
-        TP,
-        scatter_dimension=0,
-        tiled=True,
-    )
-    returned = lax.all_to_all(summed, "sp", split_axis=0, concat_axis=0, tiled=True)
-    expert_out = lax.dot_general(
-        placing,
-        returned.reshape(groups * capacity, width),
-        (((0,), (0,)), ((), ())),
-        preferred_element_type=jnp.float32,
-    )
-    return (mixed_float + expert_out).astype(jnp.bfloat16)
+    )
+    return routed_experts(
+        normed, mixed_rows, route_group, token_gates, gate_weight, up_weight, down_weight, capacity
+    )
 
 
 def solution(mesh):

time: 389 us -> 239 us (0.61)
  Pallas kernels: 0 us -> 141 us
  waiting for transfers between devices: 173 us -> 36.8 us
  blocking collectives: 77.4 us -> 4.15 us
  local copies, waits for them, and re-layouts: 59.5 us -> 5.24 us
  matrix products: 40.9 us -> 11.8 us
  other arithmetic: 3.92 us -> 8.34 us
    pallas_call x0 -> x1, Pallas kernels: none -> 141 us  [routed_experts(): pl.pallas_call(functools.partial(expert_kernel, n_sp, n_z, cap), out_shap...]
    reduce_scatter x1 -> x0, waiting for transfers between devices: 99.2 us -> none  [per_device(): lax.psum_scatter(partial_out.reshape(pooled_rows.shape).astype(jnp.bfloat...]
    all_to_all x3 -> x0, blocking collectives: 54.9 us -> none  [the longest x1 22 us: per_device(): lax.all_to_all(send_rows, 'sp', split_axis=0, concat_axis=0, tiled=True)]
    all_gather x1 -> x0, waiting for transfers between devices: 33.3 us -> none  [per_device(): lax.all_gather(arrived_rows, TP, axis=0, tiled=True)]
    dot_general x5 -> x1, matrix products: 30 us -> 0.91 us  [routed_experts(): jnp.dot(row_hot, lane_val.reshape(-1, 128), preferred_element_type=jnp.fl...]
    reshape x5 -> x0, local copies, waits for them, and re-layouts: 20.6 us -> none  [the longest x1 18.1 us: per_device(): flat_rows = pooled_rows.reshape(-1, width)]
    all_gather x1 -> x0, blocking collectives: 18.3 us -> none  [per_device(): lax.all_gather(arrived_gates, TP, axis=0, tiled=True)]
    convert_element_type x3 -> x0, local copies, waits for them, and re-layouts: 18.1 us -> none  [the longest x1 17.7 us: per_device(): partial_out.reshape(pooled_rows.shape).astype(jnp.bfloat16)]
  transfers between devices with their start and end apart: 6 -> 4, of which waited for: 5 -> 2; matrix products, arithmetic and copies ran while one was open for 3% -> 6% of each run, Pallas kernels for 0% -> 0%
where the time goes in v1:
time: 239 us
  Pallas kernels  141 us (59%)
  waiting for transfers between devices  36.8 us (15%)
  starting transfers between devices  16.4 us (7%)
  between operations  14.4 us (6%)
  matrix products  11.8 us (5%)
  other arithmetic  8.34 us (3%)
  local copies, waits for them, and re-layouts  5.24 us (2%)
  blocking collectives  4.15 us (2%)
    pallas_call x1, Pallas kernels, routed_experts(): pl.pallas_call(functools.partial(expert_kernel, n_sp, n_z, cap), out_shap...  141 us
    all_to_all x1, waiting for transfers between devices, exchange_in_order(): lax.all_to_all(blocks, axes[k], split_axis=k, concat_axis=k, tiled=True)  21.6 us
    all_gather x1, waiting for transfers between devices, per_device(): weight_piece = lax.all_gather(out_weight, TP, axis=0, tiled=True)  14.5 us
    all_to_all x1, starting transfers between devices, exchange_in_order(): lax.all_to_all(blocks, axes[k], split_axis=k, concat_axis=k, tiled=True)  8.46 us
    dot_general x1, matrix products, per_device(): jnp.einsum('rkc,kcd->krd', columns, weight_slabs, preferred_element_type=...  5.71 us
  transfers between devices with their start and end apart: 4, of which 2 were waited for; matrix products, arithmetic and copies ran while one was open for 6% of the time, Pallas kernels for 0%

profile of v1, /device:TPU:8, one launch (start us, length us, event | category | flops | bytes accessed | tf_op | source)
XLA Modules:
  0.0 238.6 jit_solution(12447492349369440331)
XLA Ops:
  6.5 0.0 copy-start
  6.5 0.0 copy-start.5
  6.5 0.0 copy-start.7
  6.5 0.0 all-gather.2.cloned.1.call-start
  6.5 0.7 all-gather.2.cloned.1.call-update
  7.3 1.3 dynamic-slice_bitcast_fusion
  8.6 3.4 %collective-permute-start = (bf16[2,128,128]{2,1,0:T(8,128)(2,1)S(1)}, bf16[2,128,128]{2,1,0:T(8,128)(2,1)S(1)}, u32[]{:S(2)}, u32[]{:S(2)}) collective-permute-start(bf16[2,128,128]{2,1,0:T(8,128)(2,1)S(1)} %get-tuple-element.12), channel_id=1, source_target_pairs={{0,16},{16,32},{32,48},{48,64},{64,80},{80,96},{96,112},{112,128},... | collective-permute-start | bytes 196616 | tf_op jit(solution)/shard_map/ppermute | solution.py:31
  12.0 4.6 %collective-permute-start.1 = (bf16[2,128,128]{2,1,0:T(8,128)(2,1)S(1)}, bf16[2,128,128]{2,1,0:T(8,128)(2,1)S(1)}, u32[]{:S(2)}, u32[]{:S(2)}) collective-permute-start(bf16[2,128,128]{2,1,0:T(8,128)(2,1)S(1)} %get-tuple-element.13), channel_id=1, source_target_pairs={{16,0},{32,16},{48,32},{64,48},{80,64},{96,80},{112,96},{128,112},... | collective-permute-start | bytes 196616 | tf_op jit(solution)/shard_map/ppermute | solution.py:34
  17.2 0.0 copy-done.5
  17.2 0.1 fusion.17
  17.3 0.2 reduce_window_sum.11
  17.5 0.0 copy-done.7
  17.6 0.2 select_reduce_fusion
  17.8 0.7 and_convert_fusion.gate_pick
  18.5 0.1 fusion.22
  18.5 0.7 fusion.20.pick
  19.2 0.1 add_add_fusion
  19.3 0.6 fusion.19.pick_t
  19.9 0.0 collective-permute-done
  19.9 0.0 collective-permute-done.1
  19.9 0.1 pad_maximum_fusion.1
  20.0 0.8 fusion.30
  20.8 0.4 pad_maximum_fusion
  21.2 0.0 copy-done
  21.2 4.2 %fusion.31 = (f32[16,128]{1,0:T(8,128)S(1)}, f32[16,1,128,384]{2,3,0,1:T(8,128)S(1)}) fusion(bf16[16,128,128]{2,1,0:T(8,128)(2,1)S(1)} %bitcast.45, bf16[2,16,384,128]{3,2,1,0:T(8,128)(2,1)S(1)} %pad_maximum_fusion, pred[16,384]{1,0:T(8,128)(4,1)S(1)} %get-tuple-element.17, pred[16,384]{1,0:T(8,128)(4,1)S(1)} %get-tuple-element.16, ...), kind=kOutput, calls=%fused_computation.83 | convolution fusion | flops 207616000 | bytes 5296128 | tf_op jit(solution)/shard_map/nqhd,nkd->nhqk/dot_general | solution.py:93
  25.4 0.4 fusion.2
  25.8 1.0 fusion.5
  26.9 0.0 copy-start.6
  26.9 4.2 %all_to_all.10 = bf16[8,2,128,128]{2,3,0,1:T(8,128)(2,1)S(1)} all-to-all(bf16[8,2,128,128]{2,3,0,1:T(8,128)(2,1)S(1)} %copy.35), channel_id=1, replica_groups=mesh['sp'=16,'tp_0'=8,'tp_1'=2] {'tp_1'}, dimensions={1} | all-to-all | bytes 1048576 | tf_op jit(solution)/shard_map/all_to_all | solution.py:55
  31.1 0.8 copy.36
  31.9 8.5 %all-to-all-start.1 = ((bf16[8,2,128,128]{2,3,1,0:T(8,128)(2,1)}), bf16[8,2,128,128]{2,3,1,0:T(8,128)(2,1)S(1)}, u32[]{:S(2)}, u32[]{:S(2)}) async-start(bf16[8,2,128,128]{2,3,1,0:T(8,128)(2,1)} %copy.36), calls=%async_computation.1 | async-start | bytes 1048576 | tf_op jit(solution)/shard_map/all_to_all | solution.py:55
  40.4 0.0 copy-done.6
  40.4 0.7 fusion.13.placing
  41.1 0.7 fusion.14.placing_t
  41.8 0.1 fusion.18
  41.8 0.9 fusion.8.gate_rows
  42.8 21.6 %all-to-all-done.1 = bf16[8,2,128,128]{2,3,1,0:T(8,128)(2,1)S(1)} async-done(((bf16[8,2,128,128]{2,3,1,0:T(8,128)(2,1)}), bf16[8,2,128,128]{2,3,1,0:T(8,128)(2,1)S(1)}, u32[]{:S(2)}, u32[]{:S(2)}) %all-to-all-start.1) | async-done | bytes 524320 | tf_op jit(solution)/shard_map/all_to_all | solution.py:55
  64.4 0.3 copy.37
  64.6 14.5 %all-gather.2.cloned.1.call-done = bf16[2048,2048]{1,0:T(8,128)(2,1)} async-done(((bf16[128,2048]{1,0:T(8,128)(2,1)}), bf16[2048,2048]{1,0:T(8,128)(2,1)}) %all-gather.2.cloned.1.call-update) | async-done | bytes 8388624 | tf_op jit(solution)/shard_map/all_gather | solution.py:489
  79.2 5.7 %convolution_convert_fusion = bf16[16,128,2048]{2,1,0:T(8,128)(2,1)S(1)} fusion(bf16[128,16,128]{2,0,1:T(8,128)(2,1)S(1)} %bitcast.48, bf16[16,128,2048]{2,1,0:T(8,128)(2,1)} %bitcast.46), kind=kOutput, calls=%fused_computation.1 | convolution fusion | flops 1077936128 | bytes 17301504 | tf_op jit(solution)/shard_map/rkc,kcd->krd/dot_general | solution.py:494
  84.9 0.0 copy-start.2
  84.9 0.0 copy-start.3
  84.9 1.8 convert_reduce_fusion
  86.8 0.0 copy-start.4
  86.8 0.2 multiply_reduce_fusion
  86.9 0.0 copy-done.2
  86.9 0.0 copy-done.3
  86.9 0.4 fusion.9
  87.3 0.0 copy-start.1
  87.3 0.1 copy-done.4
  87.5 1.0 fusion.11.normed
  88.4 0.0 copy-done.1
  88.4 141.4 %shard_map.136 = bf16[128,2048]{1,0:T(8,128)(2,1)} custom-call(bf16[128,2048]{1,0:T(8,128)(2,1)} %fusion.11.normed, bf16[128,2048]{1,0:T(8,128)(2,1)} %copy-done.1, bf16[256,128]{1,0:T(8,128)(2,1)} %fusion.13.placing, bf16[128,256]{1,0:T(8,128)(2,1)} %fusion.14.placing_t, bf16[256,128]{1,0:T(8,128)(2,1)} %fusion.8.gate_rows, bf16[80,128]{1,0:T(8,128)(2,1)} %fusion.20.pick, ...), custom_call_target="tpu_custom_call" | custom-call | tf_op jit(solution)/shard_map/pallas_call | solution.py:424
  229.8 1.9 copy.42
  (16 shorter events, 0.2 us)
Async XLA Ops:
  6.5 14.6 %copy-start = (bf16[2048,128]{1,0:T(8,128)(2,1)S(1)}, bf16[2048,128]{1,0:T(8,128)(2,1)}, u32[]{:S(2)}) copy-start(bf16[2048,128]{1,0:T(8,128)(2,1)} %param.14) | copy-start | bytes 1572868
  6.5 10.7 %copy-start.5 = (s32[128]{0:T(128)S(1)}, s32[128]{0:T(128)}, u32[]{:S(2)}) copy-start(s32[128]{0:T(128)} %param.22) | copy-start | bytes 1540
  6.5 11.0 %copy-start.7 = (bf16[128,2]{0,1:T(2,128)(2,1)S(1)}, bf16[128,2]{0,1:T(2,128)(2,1)}, u32[]{:S(2)}) copy-start(bf16[128,2]{0,1:T(2,128)(2,1)} %param.24) | copy-start | bytes 1540
  6.5 72.6 %all-gather.2.cloned.1.call-start = ((), (), s32[]{:S(2)}) async-start(), calls=%async_computation.2 | async-start | bytes 8912896 | tf_op jit(solution)/shard_map/all_gather | solution.py:489
  8.6 11.3 %collective-permute-start = (bf16[2,128,128]{2,1,0:T(8,128)(2,1)S(1)}, bf16[2,128,128]{2,1,0:T(8,128)(2,1)S(1)}, u32[]{:S(2)}, u32[]{:S(2)}) collective-permute-start(bf16[2,128,128]{2,1,0:T(8,128)(2,1)S(1)} %get-tuple-element.12), channel_id=1, source_target_pairs={{0,16},{16,32},{32,48},{48,64},{64,80},{80,96},{96,112},{112,128},... | collective-permute-start | bytes 196616 | tf_op jit(solution)/shard_map/ppermute | solution.py:31
  12.0 7.9 %collective-permute-start.1 = (bf16[2,128,128]{2,1,0:T(8,128)(2,1)S(1)}, bf16[2,128,128]{2,1,0:T(8,128)(2,1)S(1)}, u32[]{:S(2)}, u32[]{:S(2)}) collective-permute-start(bf16[2,128,128]{2,1,0:T(8,128)(2,1)S(1)} %get-tuple-element.13), channel_id=1, source_target_pairs={{16,0},{32,16},{48,32},{64,48},{80,64},{96,80},{112,96},{128,112},... | collective-permute-start | bytes 196616 | tf_op jit(solution)/shard_map/ppermute | solution.py:34
  26.9 13.5 %copy-start.6 = (s32[128,2]{0,1:T(2,128)S(1)}, s32[128,2]{0,1:T(2,128)}, u32[]{:S(2)}) copy-start(s32[128,2]{0,1:T(2,128)} %param.23) | copy-start | bytes 3076
  31.9 32.4 %all-to-all-start.1 = ((bf16[8,2,128,128]{2,3,1,0:T(8,128)(2,1)}), bf16[8,2,128,128]{2,3,1,0:T(8,128)(2,1)S(1)}, u32[]{:S(2)}, u32[]{:S(2)}) async-start(bf16[8,2,128,128]{2,3,1,0:T(8,128)(2,1)} %copy.36), calls=%async_computation.1 | async-start | bytes 1048576 | tf_op jit(solution)/shard_map/all_to_all | solution.py:55
  84.9 2.1 copy-start.2
  84.9 2.0 copy-start.3
  86.8 0.7 copy-start.4
  87.3 1.1 copy-start.1
Sparse Core Ops, SparseCore 0:
  9.2 69.9 all-gather.1

commit v2 on v1

v2 whole, which is shorter than its diff:
```python
import functools

import jax
import jax.numpy as jnp
import numpy as np
from jax import lax
from jax.experimental import pallas as pl
from jax.experimental.pallas import tpu as pltpu
from jax.sharding import Mesh
from jax.sharding import PartitionSpec as P

HEADS = 16
KV_HEADS = 4
HEAD_DIM = 128
WINDOW = 128
BLOCK = 128
GROUP_EXPERTS = 3
GROUP_CAP = 10
SLOT = 16
TP = ("tp_0", "tp_1")
SP_TP = ("sp", "tp_0", "tp_1")
MESH_ID = pl.DeviceIdType.MESH
VMEM_LIMIT = 62 * 1024 * 1024

EPS = 1e-06
NEG_BIG = -1e30
BF = jnp.bfloat16
F32 = jnp.float32


def one_hot(condition):
    return jnp.where(condition, 1.0, 0.0).astype(BF)


def iota(shape, dim):
    return lax.broadcasted_iota(jnp.int32, shape, dim)


def layer_kernel(
    n_sp,
    n_x,
    n_z,
    kv_share,
    cap,
    queries,
    key_heads,
    value_heads,
    sink,
    out_weight,
    residual,
    mixer_gain,
    expert_gain,
    info,
    pick,
    pick_t,
    gate_pick,
    wg,
    wu,
    wd,
    out,
    q_buf,
    k_buf,
    v_buf,
    att,
    by_token,
    w_proj,
    proj,
    normed,
    mixed,
    placing,
    gate_rows,
    send,
    arr,
    rows,
    gates,
    gcol,
    hidden,
    w_in,
    w_out,
    own,
    oth,
    got,
    hop,
    ret,
    back,
    load_sem,
    halo_s,
    halo_r,
    a2a_s,
    a2a_r,
    col_s,
    col_r,
    near_s,
    near_r,
    wide_s,
    wide_r,
    wpair_s,
    wpair_r,
    w_sem,
    disp_s,
    disp_r,
    ring_s,
    ring_r,
    rgate_s,
    rgate_r,
    pair_s,
    pair_r,
    pgate_s,
    pgate_r,
    sum_s,
    sum_r,
    hop_s,
    hop_r,
    ret_s,
    ret_r,
):
    sp, z, c = lax.axis_index("sp"), lax.axis_index("tp_0"), lax.axis_index("tp_1")
    me = z * 2 + c
    n_tp = 2 * n_z
    y, x = lax.div(sp, n_x), lax.rem(sp, n_x)
    n_y = n_sp // n_x
    tok, width = residual.shape
    experts, hid = wd.shape[0], wd.shape[1]
    half = n_sp // 2
    hr = half * cap
    far = n_z // 2
    tile = 256
    sends = []

    def remote(src, dst, s_sem, r_sem, dev):
        return pltpu.make_async_remote_copy(
            src_ref=src, dst_ref=dst, send_sem=s_sem, recv_sem=r_sem, device_id=dev, device_id_type=MESH_ID
        )

    def push(src, dst, s_sem, r_sem, dev):
        copy = remote(src, dst, s_sem, r_sem, dev)
        copy.start()
        sends.append(copy)
        return copy

    partner = (sp, z, 1 - c)
    ring_dev = ((sp, lax.rem(z + 1, n_z), c), (sp, lax.rem(z + n_z - 1, n_z), c))

    seq = q_buf.shape[0]
    head_at = pl.ds(pl.multiple_of(lax.div(me, kv_share) * HEAD_DIM, HEAD_DIM), HEAD_DIM)
    inner = pl.ds(WINDOW, seq)
    col_own = pl.ds(pl.multiple_of(sp * 128, 128), 128)
    lanes_own = pl.ds(pl.multiple_of(lax.rem(x, 2) * 128, 128), 128)
    w_own = w_proj.at[y, lax.div(x, 2), z, c, :, lanes_own]
    first = [
        pltpu.make_async_copy(key_heads.at[:, head_at], k_buf.at[inner], load_sem.at[0]),
        pltpu.make_async_copy(value_heads.at[:, head_at], v_buf.at[inner], load_sem.at[1]),
        pltpu.make_async_copy(out_weight.at[:, col_own], w_own, load_sem.at[2]),
        pltpu.make_async_copy(queries, q_buf, load_sem.at[3]),
    ]
    for load in first:
        load.start()
    loads = []
    for e in range(experts):
        loads.append(pltpu.make_async_copy(wg.at[e], w_in.at[e, :, pl.ds(0, hid)], w_sem.at[e, 0]))
        loads.append(pltpu.make_async_copy(wu.at[e], w_in.at[e, :, pl.ds(hid, hid)], w_sem.at[e, 1]))
        loads.append(pltpu.make_async_copy(wd.at[e], w_out.at[pl.ds(e * hid, hid), :], w_sem.at[e, 2]))

    barrier = pltpu.get_barrier_semaphore()
    for j in range(1, n_sp):
        pl.semaphore_signal(barrier, inc=1, device_id=(lax.rem(sp + j, n_sp), z, c), device_id_type=MESH_ID)
    for j in range(1, n_tp):
        n = lax.rem(me + j, n_tp)
        pl.semaphore_signal(
            barrier, inc=1, device_id=(sp, lax.div(n, 2), lax.rem(n, 2)), device_id_type=MESH_ID
        )
    for load in first:
        load.wait()
    pl.semaphore_wait(barrier, n_sp - 1 + n_tp - 1)

    after, before = lax.rem(sp + 1, n_sp), lax.rem(sp + n_sp - 1, n_sp)
    low, high = pl.ds(0, WINDOW), pl.ds(WINDOW + seq, WINDOW)
    halo = []
    for i, buf in enumerate((k_buf, v_buf)):
        halo.append(push(buf.at[pl.ds(seq, WINDOW)], buf.at[low], halo_s.at[0, i], halo_r.at[0, i], (after, z, c)))
        halo.append(push(buf.at[pl.ds(WINDOW, WINDOW)], buf.at[high], halo_s.at[1, i], halo_r.at[1, i], (before, z, c)))

    def col_region(d):
        return w_proj.at[y, lax.div(x, 2), lax.rem(z + n_z - d, n_z), c, :, lanes_own]

    column = []
    for k in range(1, n_z):
        d = (k + 1) // 2 if k % 2 else n_z - k // 2
        push(w_own, w_own, col_s.at[d], col_r.at[d], (sp, lax.rem(z + d, n_z), c))
        column.append(d)
    for load in loads:
        load.start()

    sink_val = sink[0, 0]
    q_pos = iota((BLOCK, BLOCK + 2 * WINDOW), 0)
    k_pos = iota((BLOCK, BLOCK + 2 * WINDOW), 1)

    def attend(n):
        @pl.when(n == 0)
        def _():
            for i in range(2):
                halo[2 * i].wait_recv()

        @pl.when(n == n_tp - 1)
        def _():
            for i in range(2):
                halo[2 * i + 1].wait_recv()

        start = pl.multiple_of(n * BLOCK, BLOCK)
        keys = pl.ds(start, BLOCK + 2 * WINDOW)
        scores = lax.dot_general(
            q_buf[pl.ds(start, BLOCK), :], k_buf[keys, :], (((1,), (1,)), ((), ())), preferred_element_type=F32
        ) * HEAD_DIM ** (-0.5)
        lo = jnp.where((sp == 0) & (n == 0), WINDOW, 0)
        hi = jnp.where((sp == n_sp - 1) & (n == n_tp - 1), BLOCK + WINDOW, BLOCK + 2 * WINDOW)
        inside = (k_pos >= q_pos) & (k_pos <= q_pos + 2 * WINDOW) & (k_pos >= lo) & (k_pos < hi)
        scores = jnp.where(inside, scores, NEG_BIG)
        top = jnp.maximum(jnp.max(scores, axis=1, keepdims=True), sink_val)
        terms = jnp.exp(scores - top)
        mass = jnp.sum(terms, axis=1, keepdims=True) + jnp.exp(sink_val - top)
        value = jnp.dot(terms.astype(BF), v_buf[keys, :], preferred_element_type=F32)
        return (value / mass).astype(BF)

    my_cols = pl.ds(pl.multiple_of(me * HEAD_DIM, HEAD_DIM), HEAD_DIM)

    def a2a_copy(t, n):
        return remote(
            att.at[n], by_token.at[:, my_cols], a2a_s.at[t], a2a_r.at[t], (sp, lax.div(n, 2), lax.rem(n, 2))
        )

    def attend_pair(t, carry):
        ahead, behind = lax.rem(me + t, n_tp), lax.rem(me + n_tp - t, n_tp)
        first_val, second_val = attend(ahead), attend(behind)
        att[ahead] = first_val
        att[behind] = second_val
        a2a_copy(t, ahead).start()
        a2a_copy(n_tp - t, behind).start()
        return carry

    axis_len = (n_x, n_y)
    place = (x, y)
    zq = n_z // 4

    def plane_dev(axis, step):
        at_axis = lax.rem(place[axis] + step + axis_len[axis], axis_len[axis])
        return (y * n_x + at_axis, z, c) if axis == 0 else (at_axis * n_x + x, z, c)

    def plane_region(order, wide, d, dr, hf):
        axis = order if not wide else 1 - order
        at_axis = lax.rem(place[axis] + (axis_len[axis] - d if dr == 0 else d), axis_len[axis])
        zr = pl.ds(order * 2 * zq + hf * zq, zq)
        if wide:
            if axis == 1:
                return w_proj.at[at_axis, :, zr, c]
            lanes = pl.ds(pl.multiple_of(lax.rem(at_axis, 2) * 128, 128), 128)
            return w_proj.at[:, lax.div(at_axis, 2), zr, c, :, lanes]
        if axis == 0:
            lanes = pl.ds(pl.multiple_of(lax.rem(at_axis, 2) * 128, 128), 128)
            return w_proj.at[y, lax.div(at_axis, 2), zr, c, :, lanes]
        return w_proj.at[at_axis, lax.div(x, 2), zr, c, :, lanes_own]

    def plane_reach(order, wide, dr, hf):
        axis = order if not wide else 1 - order
        limit = axis_len[axis] // 2
        return limit if dr == hf else limit - 1

    def plane_copy(order, wide, d, dr, hf):
        axis = order if not wide else 1 - order
        region = plane_region(order, wide, d, dr, hf)
        s_sem, r_sem = (wide_s, wide_r) if wide else (near_s, near_r)
        sem = (order, dr, d, hf)
        return remote(region, region, s_sem.at[sem], r_sem.at[sem], plane_dev(axis, 1 if dr == 0 else -1))

    def plane_send(order, wide, d, dr, hf):
        if d < plane_reach(order, wide, dr, hf):
            copy = plane_copy(order, wide, d, dr, hf)
            copy.start()
            sends.append(copy)

    def plane_wait(order, wide, d, dr, hf):
        axis = order if not wide else 1 - order
        region = plane_region(order, wide, d, dr, hf)
        s_sem, r_sem = (wide_s, wide_r) if wide else (near_s, near_r)
        sem = (order, dr, d - 1, hf)
        remote(region, region, s_sem.at[sem], r_sem.at[sem], plane_dev(axis, 1 if dr == 0 else -1)).wait_recv()

    def plane_steps(order, wide):
        limit = axis_len[order if not wide else 1 - order] // 2
        steps = []
        for d in range(1, limit + 1):
            for sub in range(2):
                for dr in range(2):
                    hf = dr if sub == 0 else 1 - dr
                    if d <= plane_reach(order, wide, dr, hf):
                        steps.append((d, dr, hf))
        return steps

    wpairs = []

    def wpair_send(region, index):
        wpairs.append(push(region, region, wpair_s.at[index], wpair_r.at[index], partner))

    def wpair_wait(order, d, dr, hf, index):
        axis = 1 - order
        at_axis = lax.rem(place[axis] + (axis_len[axis] - d if dr == 0 else d), axis_len[axis])
        zr = pl.ds(order * 2 * zq + hf * zq, zq)
        if axis == 1:
            region = w_proj.at[at_axis, :, zr, 1 - c]
        else:
            lanes = pl.ds(pl.multiple_of(lax.rem(at_axis, 2) * 128, 128), 128)
            region = w_proj.at[:, lax.div(at_axis, 2), zr, 1 - c, :, lanes]
        remote(region, region, wpair_s.at[index], wpair_r.at[index], partner).wait_recv()

    split = max(1, (n_tp // 2) // 2)
    lax.fori_loop(1, 1 + split, attend_pair, 0)
    for d in column:
        remote(w_own, col_region(d), col_s.at[d], col_r.at[d], ring_dev[0]).wait_recv()
    for hf_step in range(2):
        for order in range(2):
            for dr in range(2):
                plane_send(order, False, 0, dr, dr if hf_step == 0 else 1 - dr)
    lax.fori_loop(1 + split, n_tp // 2, attend_pair, 0)
    opposite = lax.rem(me + n_tp // 2, n_tp)
    first_val, own_val = attend(opposite), attend(me)
    att[opposite] = first_val
    by_token[:, my_cols] = own_val
    a2a_copy(n_tp // 2, opposite).start()

    for step in plane_steps(0, False):
        for order in range(2):
            d, dr, hf = step
            plane_wait(order, False, d, dr, hf)
            plane_send(order, False, d, dr, hf)
    for hf_step in range(2):
        for order in range(2):
            for dr in range(2):
                plane_send(order, True, 0, dr, dr if hf_step == 0 else 1 - dr)
    for order in range(2):
        for hf in range(2):
            wpair_send(plane_region(order, True, 0, 0, hf), (order, hf, 0))

    group = info[0:1, :].astype(jnp.int32)
    ahead = group - sp
    ahead = jnp.where(ahead < 0, ahead + n_sp, ahead)
    chosen = iota((n_sp, tok), 0) == ahead
    earlier = one_hot(iota((tok, tok), 0) < iota((tok, tok), 1))
    ranks = jnp.dot(one_hot(chosen), earlier, preferred_element_type=F32)
    rank = jnp.sum(jnp.where(chosen, ranks, 0.0), axis=0, keepdims=True).astype(jnp.int32)
    slot_row = iota((n_sp * SLOT, tok), 0)
    placing[...] = one_hot(slot_row == ahead * SLOT + rank)
    in_half = jnp.where(ahead >= half, ahead - half, ahead)
    lane_hot = one_hot(iota((128, tok), 0) == in_half * cap + rank)
    gate_at = jnp.zeros((n_sp * SLOT, tok), F32)
    for k in range(2):
        member = info[1 + k : 2 + k, :].astype(jnp.int32)
        gate_at = gate_at + jnp.where(slot_row == ahead * SLOT + cap + member, info[3 + k : 4 + k, :], 0.0)
    gate_rows[...] = lax.dot_general(
        gate_at.astype(BF), lane_hot, (((1,), (1,)), ((), ())), preferred_element_type=F32
    )

    for step in plane_steps(0, True):
        for order in range(2):
            d, dr, hf = step
            plane_wait(order, True, d, dr, hf)
            plane_send(order, True, d, dr, hf)
            index = (order, hf, 1 + (d - 1) * 2 + dr)
            wpair_send(plane_region(order, True, d, dr, hf), index)
    for t in range(1, n_tp):
        source = pl.ds(pl.multiple_of(lax.rem(me + n_tp - t, n_tp) * HEAD_DIM, HEAD_DIM), HEAD_DIM)
        remote(att.at[0], by_token.at[:, source], a2a_s.at[t], a2a_r.at[t], partner).wait_recv()
    for order in range(2):
        for hf in range(2):
            wpair_wait(order, 0, 0, hf, (order, hf, 0))
    for d, dr, hf in plane_steps(0, True):
        for order in range(2):
            wpair_wait(order, d, dr, hf, (order, hf, 1 + (d - 1) * 2 + dr))

    w_tiles = width // tile

    def project(i, carry):
        block = w_proj[lax.div(i, w_tiles // n_y), lax.rem(i, w_tiles // n_y)].reshape(n_tp * HEAD_DIM, tile)
        columns = pl.ds(pl.multiple_of(i * tile, tile), tile)
        proj[:, columns] = jnp.dot(by_token[...], block, preferred_element_type=F32)
        return carry

    lax.fori_loop(0, w_tiles, project, 0)

    def norms(i, carry):
        at_rows = pl.ds(pl.multiple_of(i * 16, 16), 16)
        value = proj[at_rows, :]
        scale = lax.rsqrt(jnp.mean(value * value, axis=1, keepdims=True) + EPS)
        mixed_bf = (residual[at_rows, :].astype(F32) + mixer_gain[...] * (value * scale)).astype(BF)
        mixed[at_rows, :] = mixed_bf
        mixed_f = mixed_bf.astype(F32)
        scale = lax.rsqrt(jnp.mean(mixed_f * mixed_f, axis=1, keepdims=True) + EPS)
        normed[at_rows, :] = (mixed_f * scale * expert_gain[...]).astype(BF)
        return carry

    lax.fori_loop(0, tok // 16, norms, 0)

    head = jnp.dot(placing[...], normed[:, 0:128], preferred_element_type=F32)
    send[:, 0:128] = (head + gate_rows[...]).astype(BF)
    send[:, 128:] = jnp.dot(placing[...], normed[:, 128:], preferred_element_type=F32).astype(BF)
    disp = [None]
    for j in range(1, n_sp):
        block = pl.ds(j * SLOT, SLOT)
        disp.append(
            push(send.at[block], arr.at[block], disp_s.at[j], disp_r.at[j], (lax.rem(sp + j, n_sp), z, c))
        )
    arr[0:SLOT] = send[0:SLOT]

    def reach(dr, hf):
        return far if dr == hf else far - 1

    def at(dr, d):
        return (n_z - d) % n_z if dr == 0 else d

    def part(rc, hf):
        return pl.ds((rc * 2 + hf) * hr, hr)

    ring = {}
    ring_g = {}
    pair = {}

    def ring_send(dr, d, hf):
        src, dst = at(dr, d), at(dr, d + 1)
        sem = (dr, d, hf)
        ring[sem] = push(
            rows.at[src, part(0, hf)], rows.at[dst, part(0, hf)], ring_s.at[sem], ring_r.at[sem], ring_dev[dr]
        )
        ring_g[sem] = push(
            gates.at[src, 0, hf], gates.at[dst, 0, hf], rgate_s.at[sem], rgate_r.at[sem], ring_dev[dr]
        )

    def ring_wait(dr, d, hf):
        ring[(dr, d - 1, hf)].wait_recv()
        ring_g[(dr, d - 1, hf)].wait_recv()

    def pair_send(o, hf):
        pair[(o, hf)] = (
            push(rows.at[o, part(0, hf)], rows.at[o, part(1, hf)], pair_s.at[o, hf], pair_r.at[o, hf], partner),
            push(gates.at[o, 0, hf], gates.at[o, 1, hf], pgate_s.at[o, hf], pgate_r.at[o, hf], partner),
        )

    for hf in range(2):
        for j in range(hf * half, (hf + 1) * half):
            if j > 0:
                disp[j].wait_recv()
        block = pl.ds(hf * half * SLOT, half * SLOT)
        rows[0, part(0, hf)] = jnp.dot(pick[...], arr[block, :], preferred_element_type=F32).astype(BF)
        gates[0, 0, hf] = jnp.dot(
            gate_pick[...], arr[block, 0:128], preferred_element_type=F32
        ).astype(BF)
        ring_send(0, 0, hf)
        ring_send(1, 0, hf)
        pair_send(0, hf)

    for load in loads:
        load.wait()

    eye = one_hot(iota((hr, 128), 0) == iota((hr, 128), 1))
    summed = {}

    def compute(o):
        for hf in range(2):
            for copy in pair[(o, hf)]:
                copy.wait_recv()
        for rc in range(2):
            for hf in range(2):
                gcol[part(rc, hf)] = lax.dot_general(
                    eye, gates[o, rc, hf], (((1,), (1,)), ((), ())), preferred_element_type=F32
                )
        for e in range(experts):
            pre = jnp.dot(rows[o], w_in[e], preferred_element_type=F32)
            gate_pre, up_pre = pre[:, :hid], pre[:, hid:]
            scaled = gate_pre / (1.0 + jnp.exp(-gate_pre)) * up_pre * gcol[:, e : e + 1]
            hidden[:, e * hid : (e + 1) * hid] = scaled.astype(BF)

        def down(i, carry):
            columns = pl.ds(pl.multiple_of(i * tile, tile), tile)
            piece = jnp.dot(hidden[...], w_out[:, columns], preferred_element_type=F32).astype(
                BF
            )
            own[o, :, columns] = piece[: 2 * hr]
            oth[o, :, columns] = piece[2 * hr :]
            return carry

        lax.fori_loop(0, width // tile, down, 0)
        summed[o] = push(oth.at[o], got.at[o], sum_s.at[o], sum_r.at[o], partner)

    hops = {}
    settled = set()

    def settle(o):
        if o not in settled:
            summed[o].wait_recv()
            settled.add(o)

    def half_rows(hf, i):
        return pl.ds(pl.multiple_of(hf * hr + i * 16, 16), 16)

    def hop_send(dr, d, hf):
        o = (n_z - d) % n_z if dr == 1 else d
        settle(o)
        start = d == reach(dr, hf)
        if start:
            src = own.at[o, pl.ds(hf * hr, hr)]
        else:
            hops[(dr, d + 1, hf)].wait_recv()
            src = hop.at[dr, d, hf]

        def add(i, carry):
            local = pl.ds(pl.multiple_of(i * 16, 16), 16)
            total = own[o, half_rows(hf, i)].astype(F32) + got[o, half_rows(hf, i)].astype(F32)
            if not start:
                total = total + hop[dr, d, hf, local].astype(F32)
            src[local] = total.astype(BF)
            return carry

        lax.fori_loop(0, hr // 16, add, 0)
        sem = (dr, d, hf)
        hops[sem] = push(src, hop.at[dr, d - 1, hf], hop_s.at[sem], hop_r.at[sem], ring_dev[dr])

    compute(0)
    order = []
    for d in range(1, far):
        order += [(d, 0), (d, 1)]
    for d, sub in order:
        for dr in range(2):
            hf = sub
            ring_wait(dr, d, hf)
            if d < reach(dr, hf):
                ring_send(dr, d, hf)
            pair_send(at(dr, d), hf)
        if sub == 1:
            compute(at(0, d))
            compute(at(1, d))
    for dr in range(2):
        hop_send(dr, far - 1, 1 - dr)
    for dr in range(2):
        ring_wait(dr, far, dr)
        pair_send(at(dr, far), dr)
    compute(far)
    for dr in range(2):
        hop_send(dr, far, dr)
    for d in range(far - 2, 0, -1):
        for dr in range(2):
            hop_send(dr, d, 1 - dr)
        for dr in range(2):
            hop_send(dr, d + 1, dr)
    for dr in range(2):
        hop_send(dr, 1, dr)

    settle(0)
    returned = [None] * n_sp
    for hf in range(2):
        for dr in range(2):
            hops[(dr, 1, hf)].wait_recv()

        def finish(i, carry):
            local = pl.ds(pl.multiple_of(i * 16, 16), 16)
            total = own[0, half_rows(hf, i)].astype(F32) + got[0, half_rows(hf, i)].astype(F32)
            total = total + (hop[0, 0, hf, local].astype(F32) + hop[1, 0, hf, local].astype(F32))
            own[0, half_rows(hf, i)] = total.astype(BF)
            return carry

        lax.fori_loop(0, hr // 16, finish, 0)
        ret[pl.ds(hf * half * SLOT, half * SLOT)] = jnp.dot(
            pick_t[...], own[0, pl.ds(hf * hr, hr)], preferred_element_type=F32
        ).astype(BF)
        for j in range(hf * half, (hf + 1) * half):
            block = pl.ds(j * SLOT, SLOT)
            if j == 0:
                back[block] = ret[block]
            else:
                returned[j] = push(
                    ret.at[block], back.at[block], ret_s.at[j], ret_r.at[j], (lax.rem(sp + n_sp - j, n_sp), z, c)
                )
    for j in range(1, n_sp):
        returned[j].wait_recv()
    eye_tok = one_hot(iota((tok, tok), 0) == iota((tok, tok), 1))
    placing_t = lax.dot_general(eye_tok, placing[...], (((1,), (1,)), ((), ())), preferred_element_type=F32)
    expert_out = jnp.dot(placing_t.astype(BF), back[...], preferred_element_type=F32)
    out[...] = (mixed[...].astype(F32) + expert_out).astype(BF)
    for t in range(1, n_tp):
        a2a_copy(t, lax.rem(me + t, n_tp)).wait_send()
    for copy in sends:
        copy.wait_send()


def per_device(
    queries,
    key_heads,
    value_heads,
    sink_logit,
    out_weight,
    residual,
    mixer_gain,
    expert_gain,
    route_group,
    route_member,
    route_weight,
    gate_weight,
    up_weight,
    down_weight,
    n_x=4,
    cap=GROUP_CAP,
    kv_share=HEADS // KV_HEADS,
):
    n_sp, n_z = lax.axis_size("sp"), lax.axis_size("tp_0")
    n_y = n_sp // n_x
    n_tp = 2 * n_z
    tok, width = residual.shape
    seq = queries.shape[0]
    experts, hid = down_weight.shape[0], down_weight.shape[1]
    half = n_sp // 2
    hr = half * cap
    far = n_z // 2
    info = jnp.concatenate(
        [
            route_group.astype(F32)[None, :],
            route_member.astype(F32).T,
            route_weight.astype(F32).T,
            jnp.zeros((3, tok), F32),
        ],
        axis=0,
    )
    r = np.arange(hr)
    padded = r // cap * SLOT + r % cap
    i = np.arange(half * SLOT)
    e = np.arange(16)
    pick = jnp.asarray(i[None, :] == padded[:, None], BF)
    pick_t = jnp.asarray(i[:, None] == padded[None, :], BF)
    gate_pick = jnp.asarray((i[None, :] % SLOT == e[:, None] + cap) & (e[:, None] < experts), BF)
    vmem = pl.BlockSpec(memory_space=pltpu.VMEM)
    anywhere = pl.BlockSpec(memory_space=pl.ANY)
    dma = pltpu.SemaphoreType.DMA
    bf_bufs = [
        (seq, HEAD_DIM),
        (seq + 2 * WINDOW, HEAD_DIM),
        (seq + 2 * WINDOW, HEAD_DIM),
        (n_tp, BLOCK, HEAD_DIM),
        (tok, n_tp * HEAD_DIM),
        (n_y, n_x // 2, n_z, 2, 128, 256),
        None,
        (tok, width),
        (tok, width),
        (n_sp * SLOT, tok),
        None,
        (n_sp * SLOT, width),
        (n_sp * SLOT, width),
        (n_z, 4 * hr, width),
        (n_z, 2, 2, 16, 128),
        None,
        (4 * hr, experts * hid),
        (experts, width, 2 * hid),
        (experts * hid, width),
        (n_z, 2 * hr, width),
        (n_z, 2 * hr, width),
        (n_z, 2 * hr, width),
        (2, far, 2, hr, width),
        (n_sp * SLOT, width),
        (n_sp * SLOT, width),
    ]
    f32_bufs = iter([(tok, width), (n_sp * SLOT, 128), (4 * hr, 16)])
    buffers = [pltpu.VMEM(s, BF) if s is not None else pltpu.VMEM(next(f32_bufs), F32) for s in bf_bufs]
    sems = [(4,)]
    sems += [(2, 2)] * 2 + [(n_tp,)] * 2 + [(n_z,)] * 2 + [(2, 2, 2, 2)] * 4 + [(2, 2, 5)] * 2
    sems += [(experts, 3)] + [(n_sp,)] * 2 + [(2, far, 2)] * 4 + [(n_z, 2)] * 4 + [(n_z,)] * 2
    sems += [(2, far + 1, 2)] * 2 + [(n_sp,)] * 2
    return pl.pallas_call(
        functools.partial(layer_kernel, n_sp, n_x, n_z, kv_share, cap),
        out_shape=jax.ShapeDtypeStruct((tok, width), BF),
        in_specs=[anywhere] * 3 + [vmem, anywhere] + [vmem] * 7 + [anywhere] * 3,
        out_specs=vmem,
        scratch_shapes=buffers + [dma(s) for s in sems],
        compiler_params=pltpu.CompilerParams(
            collective_id=0, has_side_effects=True, vmem_limit_bytes=VMEM_LIMIT
        ),
    )(
        queries,
        key_heads,
        value_heads,
        sink_logit.reshape(1, 1),
        out_weight,
        residual,
        mixer_gain.reshape(1, -1),
        expert_gain.reshape(1, -1),
        info,
        pick,
        pick_t,
        gate_pick,
        gate_weight,
        up_weight,
        down_weight,
    )


def solution(mesh):
    torus = Mesh(mesh.devices.reshape(mesh.shape["sp"], 8, 2), ("sp", "tp_0", "tp_1"))
    placed = (
        P("sp", TP),
        P("sp", None),
        P("sp", None),
        P(TP),
        P(TP, None),
        P(SP_TP, None),
        P(),
        P(),
        P(SP_TP),
        P(SP_TP, None),
        P(SP_TP, None),
        P("sp", None, TP),
        P("sp", None, TP),
        P("sp", TP, None),
    )
    return jax.shard_map(
        per_device, mesh=torus, in_specs=placed, out_specs=P(SP_TP, None), check_vma=False
    )
```

time: 239 us -> 197 us (0.82)
  Pallas kernels: 141 us -> 191 us
  waiting for transfers between devices: 36.8 us -> 0 us
  starting transfers between devices: 16.4 us -> 0 us
  between operations: 14.4 us -> 0.66 us
  matrix products: 11.8 us -> 0 us
  other arithmetic: 8.34 us -> 2.66 us
  blocking collectives: 4.15 us -> 0 us
  local copies, waits for them, and re-layouts: 5.24 us -> 1.96 us
    pallas_call x1, Pallas kernels: 141 us -> 191 us  [per_device(): pl.pallas_call(functools.partial(layer_kernel, n_sp, n_x, n_z, kv_share,...]
    all_to_all x1 -> x0, waiting for transfers between devices: 21.6 us -> none  [exchange_in_order(): lax.all_to_all(blocks, axes[k], split_axis=k, concat_axis=k, tiled=True)]
    all_gather x1 -> x0, waiting for transfers between devices: 14.5 us -> none  [per_device(): weight_piece = lax.all_gather(out_weight, TP, axis=0, tiled=True)]
    dot_general x4 -> x0, matrix products: 11.8 us -> none  [the longest x1 5.71 us: per_device(): jnp.einsum('rkc,kcd->krd', columns, weight_slabs, preferred_element_type=...]
    all_to_all x1 -> x0, starting transfers between devices: 8.46 us -> none  [exchange_in_order(): lax.all_to_all(blocks, axes[k], split_axis=k, concat_axis=k, tiled=True)]
    ppermute x2 -> x0, starting transfers between devices: 7.95 us -> none  [the longest x1 4.55 us: extended(): lax.ppermute(lax.slice_in_dim(block, 0, width, axis=dim), axis, backward)]
    convert_element_type x9 -> x0, other arithmetic: 4.46 us -> none  [the longest x1 0.98 us: per_device(): normed = (mixed_float * norm_scale * expert_gain).astype(jnp.bfloat16)]
    all_to_all x1 -> x0, blocking collectives: 4.15 us -> none  [exchange_in_order(): lax.all_to_all(blocks, axes[k], split_axis=k, concat_axis=k, tiled=True)]
  transfers between devices with their start and end apart: 4 -> 0, of which waited for: 2 -> 0; matrix products, arithmetic and copies ran while one was open for 6% -> 0% of each run, Pallas kernels for 0% -> 0%
where the time goes in v2:
time: 197 us; the launch traced here: 196 us
  Pallas kernels  191 us (97%)
  other arithmetic  2.66 us (1%)
    pallas_call x1, Pallas kernels, per_device(): pl.pallas_call(functools.partial(layer_kernel, n_sp, n_x, n_z, kv_share,...  191 us

profile of v2, /device:TPU:8, one launch (start us, length us, event | category | flops | bytes accessed | tf_op | source)
XLA Modules:
  0.0 195.9 jit_solution(11512480985814937490)
XLA Ops:
  0.7 0.7 convert_bitcast_fusion.2
  1.3 0.1 pad.3.clone
  1.4 0.7 convert_bitcast_fusion.1
  2.1 0.7 convert_bitcast_fusion
  2.7 0.7 maximum_maximum_fusion.info
  3.4 190.6 %shard_map.163 = bf16[128,2048]{1,0:T(8,128)(2,1)} custom-call(bf16[2048,128]{1,0:T(8,128)(2,1)} %queries.1, bf16[2048,512]{1,0:T(8,128)(2,1)} %key_heads.1, bf16[2048,512]{1,0:T(8,128)(2,1)} %value_heads.1, f32[1,1]{1,0:T(1,128)} %bitcast.9.sink, bf16[128,2048]{1,0:T(8,128)(2,1)} %out_weight.1, bf16[128,2048]{1,0:T(8,128)(2,1)} %residual.1, ...), custom_call_target="tpu_custom_call" | custom-call | tf_op jit(solution)/shard_map/pallas_call | solution.py:671
  194.0 1.9 copy.20
  (1 shorter events, 0.0 us)

commit v3 on v2

--- a/solution.py
+++ b/solution.py
@@ -17,6 +17,7 @@
 GROUP_EXPERTS = 3
 GROUP_CAP = 10
 SLOT = 16
+CHUNKS = 4
 TP = ("tp_0", "tp_1")
 SP_TP = ("sp", "tp_0", "tp_1")
 MESH_ID = pl.DeviceIdType.MESH
@@ -50,7 +51,9 @@
     residual,
     mixer_gain,
     expert_gain,
-    info,
+    route_group,
+    route_member,
+    route_weight,
     pick,
     pick_t,
     gate_pick,
@@ -125,6 +128,7 @@
     hr = half * cap
     far = n_z // 2
     tile = 256
+    span = width // CHUNKS
     sends = []
 
     def remote(src, dst, s_sem, r_sem, dev):
@@ -339,8 +343,7 @@
         for hf in range(2):
             wpair_send(plane_region(order, True, 0, 0, hf), (order, hf, 0))
 
-    group = info[0:1, :].astype(jnp.int32)
-    ahead = group - sp
+    ahead = route_group[...] - sp
     ahead = jnp.where(ahead < 0, ahead + n_sp, ahead)
     chosen = iota((n_sp, tok), 0) == ahead
     earlier = one_hot(iota((tok, tok), 0) < iota((tok, tok), 1))
@@ -352,8 +355,9 @@
     lane_hot = one_hot(iota((128, tok), 0) == in_half * cap + rank)
     gate_at = jnp.zeros((n_sp * SLOT, tok), F32)
     for k in range(2):
-        member = info[1 + k : 2 + k, :].astype(jnp.int32)
-        gate_at = gate_at + jnp.where(slot_row == ahead * SLOT + cap + member, info[3 + k : 4 + k, :], 0.0)
+        member = route_member[k : k + 1, :]
+        weight = route_weight[k : k + 1, :].astype(F32)
+        gate_at = gate_at + jnp.where(slot_row == ahead * SLOT + cap + member, weight, 0.0)
     gate_rows[...] = lax.dot_general(
         gate_at.astype(BF), lane_hot, (((1,), (1,)), ((), ())), preferred_element_type=F32
     )
@@ -401,12 +405,22 @@
     head = jnp.dot(placing[...], normed[:, 0:128], preferred_element_type=F32)
     send[:, 0:128] = (head + gate_rows[...]).astype(BF)
     send[:, 128:] = jnp.dot(placing[...], normed[:, 128:], preferred_element_type=F32).astype(BF)
-    disp = [None]
-    for j in range(1, n_sp):
-        block = pl.ds(j * SLOT, SLOT)
-        disp.append(
-            push(send.at[block], arr.at[block], disp_s.at[j], disp_r.at[j], (lax.rem(sp + j, n_sp), z, c))
-        )
+    def cut(ch):
+        return pl.ds(ch * span, span)
+
+    disp = {}
+    for hf in range(2):
+        for ch in range(CHUNKS):
+            for j in range(hf * half, (hf + 1) * half):
+                at_slot = (pl.ds(j * SLOT, SLOT), cut(ch))
+                if j > 0:
+                    disp[(ch, j)] = push(
+                        send.at[at_slot],
+                        arr.at[at_slot],
+                        disp_s.at[ch, j],
+                        disp_r.at[ch, j],
+                        (lax.rem(sp + j, n_sp), z, c),
+                    )
     arr[0:SLOT] = send[0:SLOT]
 
     def reach(dr, hf):
@@ -415,44 +429,66 @@
     def at(dr, d):
         return (n_z - d) % n_z if dr == 0 else d
 
-    def part(rc, hf):
-        return pl.ds((rc * 2 + hf) * hr, hr)
+    arrivals = [(1, 0), (1, 1)] + [(d, 0) for d in range(2, far + 1)] + [(d, 1) for d in range(2, far)]
+    together = [[(0, 0), (0, 1)]]
+    for d, kind in arrivals:
+        together.append([(at(dr, d), kind if d == 1 or dr == 0 else 1 - kind) for dr in range(2)])
+    place_at = {unit: (i, sub) for i, units in enumerate(together) for sub, unit in enumerate(units)}
+
+    def spot(o, rc, hf):
+        i, sub = place_at[(o, hf)]
+        return i, pl.ds((sub * 2 + rc) * hr, hr)
+
+    def sum_spot(o, hf):
+        i, sub = place_at[(o, hf)]
+        return i, pl.ds(sub * hr, hr)
 
     ring = {}
     ring_g = {}
     pair = {}
 
-    def ring_send(dr, d, hf):
+    def ring_send(dr, d, hf, ch):
         src, dst = at(dr, d), at(dr, d + 1)
-        sem = (dr, d, hf)
+        sem = (dr, d, hf, ch)
         ring[sem] = push(
-            rows.at[src, part(0, hf)], rows.at[dst, part(0, hf)], ring_s.at[sem], ring_r.at[sem], ring_dev[dr]
+            rows.at[(*spot(src, 0, hf), cut(ch))],
+            rows.at[(*spot(dst, 0, hf), cut(ch))],
+            ring_s.at[sem],
+            ring_r.at[sem],
+            ring_dev[dr],
         )
-        ring_g[sem] = push(
-            gates.at[src, 0, hf], gates.at[dst, 0, hf], rgate_s.at[sem], rgate_r.at[sem], ring_dev[dr]
-        )
-
-    def ring_wait(dr, d, hf):
-        ring[(dr, d - 1, hf)].wait_recv()
-        ring_g[(dr, d - 1, hf)].wait_recv()
+        if ch == 0:
+            sem = (dr, d, hf)
+            ring_g[sem] = push(
+                gates.at[src, 0, hf], gates.at[dst, 0, hf], rgate_s.at[sem], rgate_r.at[sem], ring_dev[dr]
+            )
+
+    def ring_wait(dr, d, hf, ch):
+        ring[(dr, d - 1, hf, ch)].wait_recv()
+        if ch == 0:
+            ring_g[(dr, d - 1, hf)].wait_recv()
 
     def pair_send(o, hf):
         pair[(o, hf)] = (
-            push(rows.at[o, part(0, hf)], rows.at[o, part(1, hf)], pair_s.at[o, hf], pair_r.at[o, hf], partner),
+            push(rows.at[spot(o, 0, hf)], rows.at[spot(o, 1, hf)], pair_s.at[o, hf], pair_r.at[o, hf], partner),
             push(gates.at[o, 0, hf], gates.at[o, 1, hf], pgate_s.at[o, hf], pgate_r.at[o, hf], partner),
         )
 
     for hf in range(2):
-        for j in range(hf * half, (hf + 1) * half):
-            if j > 0:
-                disp[j].wait_recv()
         block = pl.ds(hf * half * SLOT, half * SLOT)
-        rows[0, part(0, hf)] = jnp.dot(pick[...], arr[block, :], preferred_element_type=F32).astype(BF)
-        gates[0, 0, hf] = jnp.dot(
-            gate_pick[...], arr[block, 0:128], preferred_element_type=F32
-        ).astype(BF)
-        ring_send(0, 0, hf)
-        ring_send(1, 0, hf)
+        for ch in range(CHUNKS):
+            for j in range(hf * half, (hf + 1) * half):
+                if j > 0:
+                    disp[(ch, j)].wait_recv()
+            if ch == 0:
+                gates[0, 0, hf] = jnp.dot(
+                    gate_pick[...], arr[block, 0:128], preferred_element_type=F32
+                ).astype(BF)
+            rows[(*spot(0, 0, hf), cut(ch))] = jnp.dot(
+                pick[...], arr[block, cut(ch)], preferred_element_type=F32
+            ).astype(BF)
+            ring_send(0, 0, hf, ch)
+            ring_send(1, 0, hf, ch)
         pair_send(0, hf)
 
     for load in loads:
@@ -461,127 +497,175 @@
     eye = one_hot(iota((hr, 128), 0) == iota((hr, 128), 1))
     summed = {}
 
-    def compute(o):
-        for hf in range(2):
+    def compute(step):
+        for sub, (o, hf) in enumerate(together[step]):
             for copy in pair[(o, hf)]:
                 copy.wait_recv()
-        for rc in range(2):
-            for hf in range(2):
-                gcol[part(rc, hf)] = lax.dot_general(
+            for rc in range(2):
+                gcol[pl.ds((sub * 2 + rc) * hr, hr)] = lax.dot_general(
                     eye, gates[o, rc, hf], (((1,), (1,)), ((), ())), preferred_element_type=F32
                 )
         for e in range(experts):
-            pre = jnp.dot(rows[o], w_in[e], preferred_element_type=F32)
+            pre = jnp.dot(rows[step], w_in[e], preferred_element_type=F32)
             gate_pre, up_pre = pre[:, :hid], pre[:, hid:]
             scaled = gate_pre / (1.0 + jnp.exp(-gate_pre)) * up_pre * gcol[:, e : e + 1]
             hidden[:, e * hid : (e + 1) * hid] = scaled.astype(BF)
 
         def down(i, carry):
             columns = pl.ds(pl.multiple_of(i * tile, tile), tile)
-            piece = jnp.dot(hidden[...], w_out[:, columns], preferred_element_type=F32).astype(
-                BF
-            )
-            own[o, :, columns] = piece[: 2 * hr]
-            oth[o, :, columns] = piece[2 * hr :]
+            piece = jnp.dot(hidden[...], w_out[:, columns], preferred_element_type=F32).astype(BF)
+            for sub in range(2):
+                own[step, pl.ds(sub * hr, hr), columns] = piece[sub * 2 * hr : (sub * 2 + 1) * hr]
+                oth[step, pl.ds(sub * hr, hr), columns] = piece[(sub * 2 + 1) * hr : (sub * 2 + 2) * hr]
             return carry
 
         lax.fori_loop(0, width // tile, down, 0)
-        summed[o] = push(oth.at[o], got.at[o], sum_s.at[o], sum_r.at[o], partner)
+        summed[step] = push(oth.at[step], got.at[step], sum_s.at[step], sum_r.at[step], partner)
 
     hops = {}
     settled = set()
 
-    def settle(o):
-        if o not in settled:
-            summed[o].wait_recv()
-            settled.add(o)
-
-    def half_rows(hf, i):
-        return pl.ds(pl.multiple_of(hf * hr + i * 16, 16), 16)
-
-    def hop_send(dr, d, hf):
+    def settle(o, hf):
+        step = place_at[(o, hf)][0]
+        if step not in settled:
+            summed[step].wait_recv()
+            settled.add(step)
+
+    def own_rows(o, hf, i):
+        step, sub = place_at[(o, hf)]
+        return step, pl.ds(pl.multiple_of(sub * hr + i * 16, 16), 16)
+
+    def hop_send(dr, d, hf, ch):
         o = (n_z - d) % n_z if dr == 1 else d
-        settle(o)
-        start = d == reach(dr, hf)
+        settle(o, hf)
+        start = d == reach(1 - dr, hf)
         if start:
-            src = own.at[o, pl.ds(hf * hr, hr)]
+            src = own.at[(*sum_spot(o, hf), cut(ch))]
         else:
-            hops[(dr, d + 1, hf)].wait_recv()
-            src = hop.at[dr, d, hf]
+            hops[(dr, d + 1, hf, ch)].wait_recv()
+            src = hop.at[dr, d, hf, :, cut(ch)]
 
         def add(i, carry):
             local = pl.ds(pl.multiple_of(i * 16, 16), 16)
-            total = own[o, half_rows(hf, i)].astype(F32) + got[o, half_rows(hf, i)].astype(F32)
+            at_rows = (*own_rows(o, hf, i), cut(ch))
+            total = own[at_rows].astype(F32) + got[at_rows].astype(F32)
             if not start:
-                total = total + hop[dr, d, hf, local].astype(F32)
+                total = total + hop[dr, d, hf, local, cut(ch)].astype(F32)
             src[local] = total.astype(BF)
             return carry
 
         lax.fori_loop(0, hr // 16, add, 0)
-        sem = (dr, d, hf)
-        hops[sem] = push(src, hop.at[dr, d - 1, hf], hop_s.at[sem], hop_r.at[sem], ring_dev[dr])
+        sem = (dr, d, hf, ch)
+        hops[sem] = push(src, hop.at[dr, d - 1, hf, :, cut(ch)], hop_s.at[sem], hop_r.at[sem], ring_dev[dr])
+
+    returned = {}
+
+    def finish(ch):
+        for hf in range(2):
+            settle(0, hf)
+            for dr in range(2):
+                hops[(dr, 1, hf, ch)].wait_recv()
+
+            def last_add(i, carry):
+                local = pl.ds(pl.multiple_of(i * 16, 16), 16)
+                at_rows = (*own_rows(0, hf, i), cut(ch))
+                total = own[at_rows].astype(F32) + got[at_rows].astype(F32)
+                total = total + (
+                    hop[0, 0, hf, local, cut(ch)].astype(F32) + hop[1, 0, hf, local, cut(ch)].astype(F32)
+                )
+                own[at_rows] = total.astype(BF)
+                return carry
+
+            lax.fori_loop(0, hr // 16, last_add, 0)
+            ret[pl.ds(hf * half * SLOT, half * SLOT), cut(ch)] = jnp.dot(
+                pick_t[...], own[(*sum_spot(0, hf), cut(ch))], preferred_element_type=F32
+            ).astype(BF)
+            for j in range(hf * half, (hf + 1) * half):
+                at_slot = (pl.ds(j * SLOT, SLOT), cut(ch))
+                if j == 0:
+                    back[0:SLOT, cut(ch)] = ret[0:SLOT, cut(ch)]
+                else:
+                    returned[(ch, j)] = push(
+                        ret.at[at_slot],
+                        back.at[at_slot],
+                        ret_s.at[ch, j],
+                        ret_r.at[ch, j],
+                        (lax.rem(sp + n_sp - j, n_sp), z, c),
+                    )
 
     compute(0)
-    order = []
-    for d in range(1, far):
-        order += [(d, 0), (d, 1)]
-    for d, sub in order:
+
+    def long_hop(d, ch):
         for dr in range(2):
-            hf = sub
-            ring_wait(dr, d, hf)
-            if d < reach(dr, hf):
-                ring_send(dr, d, hf)
-            pair_send(at(dr, d), hf)
-        if sub == 1:
-            compute(at(0, d))
-            compute(at(1, d))
-    for dr in range(2):
-        hop_send(dr, far - 1, 1 - dr)
-    for dr in range(2):
-        ring_wait(dr, far, dr)
-        pair_send(at(dr, far), dr)
-    compute(far)
-    for dr in range(2):
-        hop_send(dr, far, dr)
-    for d in range(far - 2, 0, -1):
-        for dr in range(2):
-            hop_send(dr, d, 1 - dr)
-        for dr in range(2):
-            hop_send(dr, d + 1, dr)
-    for dr in range(2):
-        hop_send(dr, 1, dr)
-
-    settle(0)
-    returned = [None] * n_sp
-    for hf in range(2):
-        for dr in range(2):
-            hops[(dr, 1, hf)].wait_recv()
-
-        def finish(i, carry):
-            local = pl.ds(pl.multiple_of(i * 16, 16), 16)
-            total = own[0, half_rows(hf, i)].astype(F32) + got[0, half_rows(hf, i)].astype(F32)
-            total = total + (hop[0, 0, hf, local].astype(F32) + hop[1, 0, hf, local].astype(F32))
-            own[0, half_rows(hf, i)] = total.astype(BF)
-            return carry
-
-        lax.fori_loop(0, hr // 16, finish, 0)
-        ret[pl.ds(hf * half * SLOT, half * SLOT)] = jnp.dot(
-            pick_t[...], own[0, pl.ds(hf * hr, hr)], preferred_element_type=F32
-        ).astype(BF)
-        for j in range(hf * half, (hf + 1) * half):
-            block = pl.ds(j * SLOT, SLOT)
-            if j == 0:
-                back[block] = ret[block]
-            else:
-                returned[j] = push(
-                    ret.at[block], back.at[block], ret_s.at[j], ret_r.at[j], (lax.rem(sp + n_sp - j, n_sp), z, c)
-                )
-    for j in range(1, n_sp):
-        returned[j].wait_recv()
+            hop_send(dr, d, 1 - dr, ch)
+
+    done = {0}
+
+    def need(step):
+        if step not in done:
+            compute(step)
+            done.add(step)
+
+    far_step = place_at[(far, 0)][0]
+    for k, (d, kind) in enumerate(arrivals):
+        step = k + 1
+        for ch in range(CHUNKS):
+            if step == far_step + 1 and ch == CHUNKS // 2:
+                need(far_step)
+            for dr in range(2):
+                hf = together[step][dr][1]
+                ring_wait(dr, d, hf, ch)
+                if d < reach(dr, hf) and not (d == 1 and dr != hf):
+                    ring_send(dr, d, hf, ch)
+        if (d, kind) == (far - 1, 0):
+            for ch in range(CHUNKS):
+                for dr in range(2):
+                    if 1 < reach(dr, 1 - dr):
+                        ring_send(dr, 1, 1 - dr, ch)
+        for o, hf in together[step]:
+            pair_send(o, hf)
+        if k > 0 and step != far_step + 1 and step != len(arrivals):
+            need(step - 1)
+        if step == len(arrivals) - 1 and far > 2:
+            for ch in range(CHUNKS):
+                long_hop(far, ch)
+            need(step)
+    if far == 2:
+        need(1)
+        need(2)
+        need(3)
+        for ch in range(CHUNKS):
+            long_hop(far, ch)
+    for ch in range(CHUNKS // 2):
+        long_hop(far - 1, ch)
+    need(len(arrivals))
+    for ch in range(CHUNKS // 2, CHUNKS):
+        long_hop(far - 1, ch)
+    events = []
+    for ch in range(CHUNKS):
+        at_key = 1.2 * ch
+        for d in range(far - 1, 0, -1):
+            events.append((at_key, ch, d, 1))
+            at_key += 1
+            if d > 1:
+                events.append((at_key, ch, d - 1, 0))
+                at_key += 1
+        events.append((at_key + 0.3, ch, 0, 0))
+    for _, ch, d, kind in sorted(events):
+        if d == 0:
+            finish(ch)
+        else:
+            for dr in range(2):
+                hop_send(dr, d, 1 - dr if kind == 0 else dr, ch)
     eye_tok = one_hot(iota((tok, tok), 0) == iota((tok, tok), 1))
-    placing_t = lax.dot_general(eye_tok, placing[...], (((1,), (1,)), ((), ())), preferred_element_type=F32)
-    expert_out = jnp.dot(placing_t.astype(BF), back[...], preferred_element_type=F32)
-    out[...] = (mixed[...].astype(F32) + expert_out).astype(BF)
+    placing_t = lax.dot_general(
+        eye_tok, placing[...], (((1,), (1,)), ((), ())), preferred_element_type=F32
+    ).astype(BF)
+    for ch in range(CHUNKS):
+        for j in range(1, n_sp):
+            returned[(ch, j)].wait_recv()
+        expert_out = jnp.dot(placing_t, back[:, cut(ch)], preferred_element_type=F32)
+        out[:, cut(ch)] = (mixed[:, cut(ch)].astype(F32) + expert_out).astype(BF)
     for t in range(1, n_tp):
         a2a_copy(t, lax.rem(me + t, n_tp)).wait_send()
     for copy in sends:
@@ -616,15 +700,6 @@
     half = n_sp // 2
     hr = half * cap
     far = n_z // 2
-    info = jnp.concatenate(
-        [
-            route_group.astype(F32)[None, :],
-            route_member.astype(F32).T,
-            route_weight.astype(F32).T,
-            jnp.zeros((3, tok), F32),
-        ],
-        axis=0,
-    )
     r = np.arange(hr)
     padded = r // cap * SLOT + r % cap
     i = np.arange(half * SLOT)
@@ -666,12 +741,12 @@
     buffers = [pltpu.VMEM(s, BF) if s is not None else pltpu.VMEM(next(f32_bufs), F32) for s in bf_bufs]
     sems = [(4,)]
     sems += [(2, 2)] * 2 + [(n_tp,)] * 2 + [(n_z,)] * 2 + [(2, 2, 2, 2)] * 4 + [(2, 2, 5)] * 2
-    sems += [(experts, 3)] + [(n_sp,)] * 2 + [(2, far, 2)] * 4 + [(n_z, 2)] * 4 + [(n_z,)] * 2
-    sems += [(2, far + 1, 2)] * 2 + [(n_sp,)] * 2
+    sems += [(experts, 3)] + [(CHUNKS, n_sp)] * 2 + [(2, far, 2, CHUNKS)] * 2 + [(2, far, 2)] * 2 + [(n_z, 2)] * 4 + [(n_z,)] * 2
+    sems += [(2, far + 1, 2, CHUNKS)] * 2 + [(CHUNKS, n_sp)] * 2
     return pl.pallas_call(
         functools.partial(layer_kernel, n_sp, n_x, n_z, kv_share, cap),
         out_shape=jax.ShapeDtypeStruct((tok, width), BF),
-        in_specs=[anywhere] * 3 + [vmem, anywhere] + [vmem] * 7 + [anywhere] * 3,
+        in_specs=[anywhere] * 3 + [vmem, anywhere] + [vmem] * 9 + [anywhere] * 3,
         out_specs=vmem,
         scratch_shapes=buffers + [dma(s) for s in sems],
         compiler_params=pltpu.CompilerParams(
@@ -686,7 +761,9 @@
         residual,
         mixer_gain.reshape(1, -1),
         expert_gain.reshape(1, -1),
-        info,
+        route_group.reshape(1, -1),
+        route_member.T,
+        route_weight.T,
         pick,
         pick_t,
         gate_pick,

time: 197 us -> 180 us (0.914)
  Pallas kernels: 191 us -> 177 us
  other arithmetic: 2.66 us -> 0 us
    pallas_call x1, Pallas kernels: 191 us -> 177 us  [per_device(): pl.pallas_call(functools.partial(layer_kernel, n_sp, n_x, n_z, kv_share,...]
where the time goes in v3:
time: 180 us
  Pallas kernels  177 us (98%)
  local copies, waits for them, and re-layouts  1.88 us (1%)
    pallas_call x1, Pallas kernels, per_device(): pl.pallas_call(functools.partial(layer_kernel, n_sp, n_x, n_z, kv_share,...  177 us

profile of v3, /device:TPU:8, one launch (start us, length us, event | category | flops | bytes accessed | tf_op | source)
XLA Modules:
  0.0 179.9 jit_solution(2511544265610737271)
XLA Ops:
  0.7 177.4 %shard_map.163 = bf16[128,2048]{1,0:T(8,128)(2,1)} custom-call(bf16[2048,128]{1,0:T(8,128)(2,1)} %queries.1, bf16[2048,512]{1,0:T(8,128)(2,1)} %key_heads.1, bf16[2048,512]{1,0:T(8,128)(2,1)} %value_heads.1, f32[1,1]{1,0:T(1,128)} %bitcast.6.sink, bf16[128,2048]{1,0:T(8,128)(2,1)} %out_weight.1, bf16[128,2048]{1,0:T(8,128)(2,1)} %residual.1, ...), custom_call_target="tpu_custom_call" | custom-call | tf_op jit(solution)/shard_map/pallas_call | solution.py:746
  178.0 1.9 %copy.20 = bf16[128,2048]{1,0:T(8,128)(2,1)} copy(bf16[128,2048]{1,0:T(8,128)(2,1)} %shard_map.163) | data formatting | bytes 1048576

commit v4 on v3

--- a/solution.py
+++ b/solution.py
@@ -18,6 +18,7 @@
 GROUP_CAP = 10
 SLOT = 16
 CHUNKS = 4
+Z_ROWS = 32
 TP = ("tp_0", "tp_1")
 SP_TP = ("sp", "tp_0", "tp_1")
 MESH_ID = pl.DeviceIdType.MESH
@@ -99,6 +100,11 @@
     wide_r,
     wpair_s,
     wpair_r,
+    zrow_s,
+    zrow_r,
+    zpair_s,
+    zpair_r,
+    zload_sem,
     w_sem,
     disp_s,
     disp_r,
@@ -150,13 +156,24 @@
     inner = pl.ds(WINDOW, seq)
     col_own = pl.ds(pl.multiple_of(sp * 128, 128), 128)
     lanes_own = pl.ds(pl.multiple_of(lax.rem(x, 2) * 128, 128), 128)
-    w_own = w_proj.at[y, lax.div(x, 2), z, c, :, lanes_own]
+    plane_rows = pl.ds(Z_ROWS, HEAD_DIM - Z_ROWS)
+    ring_rows = pl.ds(0, Z_ROWS)
+    w_own = w_proj.at[y, lax.div(x, 2), z, c, plane_rows, lanes_own]
     first = [
         pltpu.make_async_copy(key_heads.at[:, head_at], k_buf.at[inner], load_sem.at[0]),
         pltpu.make_async_copy(value_heads.at[:, head_at], v_buf.at[inner], load_sem.at[1]),
-        pltpu.make_async_copy(out_weight.at[:, col_own], w_own, load_sem.at[2]),
+        pltpu.make_async_copy(out_weight.at[plane_rows, col_own], w_own, load_sem.at[2]),
         pltpu.make_async_copy(queries, q_buf, load_sem.at[3]),
     ]
+    for i in range(width // tile):
+        per_y = width // tile // n_y
+        first.append(
+            pltpu.make_async_copy(
+                out_weight.at[ring_rows, pl.ds(i * tile, tile)],
+                w_proj.at[i // per_y, i % per_y, z, c, ring_rows, :],
+                zload_sem.at[i],
+            )
+        )
     for load in first:
         load.start()
     loads = []
@@ -185,13 +202,33 @@
         halo.append(push(buf.at[pl.ds(WINDOW, WINDOW)], buf.at[high], halo_s.at[1, i], halo_r.at[1, i], (before, z, c)))
 
     def col_region(d):
-        return w_proj.at[y, lax.div(x, 2), lax.rem(z + n_z - d, n_z), c, :, lanes_own]
+        return w_proj.at[y, lax.div(x, 2), lax.rem(z + n_z - d, n_z), c, plane_rows, lanes_own]
 
     column = []
     for k in range(1, n_z):
         d = (k + 1) // 2 if k % 2 else n_z - k // 2
         push(w_own, w_own, col_s.at[d], col_r.at[d], (sp, lax.rem(z + d, n_z), c))
         column.append(d)
+    def zrow_reach(dr, hf):
+        return far if dr == hf else far - 1
+
+    def zrow_region(dr, d, hf):
+        at_z = lax.rem(z + (n_z - d if dr == 0 else d), n_z)
+        return w_proj.at[pl.ds(hf * (n_y // 2), n_y // 2), :, at_z, c, ring_rows, :]
+
+    def zrow_step(d):
+        for sub in range(2):
+            for dr in range(2):
+                hf = dr if sub == 0 else 1 - dr
+                region = zrow_region(dr, d, hf)
+                if 0 < d <= zrow_reach(dr, hf):
+                    sem = (dr, d - 1, hf)
+                    remote(region, region, zrow_s.at[sem], zrow_r.at[sem], ring_dev[dr]).wait_recv()
+                if d < zrow_reach(dr, hf):
+                    sem = (dr, d, hf)
+                    push(region, region, zrow_s.at[sem], zrow_r.at[sem], ring_dev[dr])
+
+    zrow_step(0)
     for load in loads:
         load.start()
 
@@ -255,13 +292,13 @@
         zr = pl.ds(order * 2 * zq + hf * zq, zq)
         if wide:
             if axis == 1:
-                return w_proj.at[at_axis, :, zr, c]
+                return w_proj.at[at_axis, :, zr, c, plane_rows]
             lanes = pl.ds(pl.multiple_of(lax.rem(at_axis, 2) * 128, 128), 128)
-            return w_proj.at[:, lax.div(at_axis, 2), zr, c, :, lanes]
+            return w_proj.at[:, lax.div(at_axis, 2), zr, c, plane_rows, lanes]
         if axis == 0:
             lanes = pl.ds(pl.multiple_of(lax.rem(at_axis, 2) * 128, 128), 128)
-            return w_proj.at[y, lax.div(at_axis, 2), zr, c, :, lanes]
-        return w_proj.at[at_axis, lax.div(x, 2), zr, c, :, lanes_own]
+            return w_proj.at[y, lax.div(at_axis, 2), zr, c, plane_rows, lanes]
+        return w_proj.at[at_axis, lax.div(x, 2), zr, c, plane_rows, lanes_own]
 
     def plane_reach(order, wide, dr, hf):
         axis = order if not wide else 1 - order
@@ -309,10 +346,10 @@
         at_axis = lax.rem(place[axis] + (axis_len[axis] - d if dr == 0 else d), axis_len[axis])
         zr = pl.ds(order * 2 * zq + hf * zq, zq)
         if axis == 1:
-            region = w_proj.at[at_axis, :, zr, 1 - c]
+            region = w_proj.at[at_axis, :, zr, 1 - c, plane_rows]
         else:
             lanes = pl.ds(pl.multiple_of(lax.rem(at_axis, 2) * 128, 128), 128)
-            region = w_proj.at[:, lax.div(at_axis, 2), zr, 1 - c, :, lanes]
+            region = w_proj.at[:, lax.div(at_axis, 2), zr, 1 - c, plane_rows, lanes]
         remote(region, region, wpair_s.at[index], wpair_r.at[index], partner).wait_recv()
 
     split = max(1, (n_tp // 2) // 2)
@@ -323,18 +360,25 @@
         for order in range(2):
             for dr in range(2):
                 plane_send(order, False, 0, dr, dr if hf_step == 0 else 1 - dr)
-    lax.fori_loop(1 + split, n_tp // 2, attend_pair, 0)
+    middle = min(3 + split, n_tp // 2)
+    lax.fori_loop(1 + split, middle, attend_pair, 0)
+
+    def near_steps(low, high):
+        for d, dr, hf in plane_steps(0, False):
+            if low <= d < high:
+                for order in range(2):
+                    plane_wait(order, False, d, dr, hf)
+                    plane_send(order, False, d, dr, hf)
+
+    zrow_step(1)
+    near_steps(1, 2)
+    lax.fori_loop(middle, n_tp // 2, attend_pair, 0)
     opposite = lax.rem(me + n_tp // 2, n_tp)
     first_val, own_val = attend(opposite), attend(me)
     att[opposite] = first_val
     by_token[:, my_cols] = own_val
     a2a_copy(n_tp // 2, opposite).start()
-
-    for step in plane_steps(0, False):
-        for order in range(2):
-            d, dr, hf = step
-            plane_wait(order, False, d, dr, hf)
-            plane_send(order, False, d, dr, hf)
+    near_steps(2, n_sp)
     for hf_step in range(2):
         for order in range(2):
             for dr in range(2):
@@ -342,6 +386,7 @@
     for order in range(2):
         for hf in range(2):
             wpair_send(plane_region(order, True, 0, 0, hf), (order, hf, 0))
+    zrow_step(2)
 
     ahead = route_group[...] - sp
     ahead = jnp.where(ahead < 0, ahead + n_sp, ahead)
@@ -362,7 +407,19 @@
         gate_at.astype(BF), lane_hot, (((1,), (1,)), ((), ())), preferred_element_type=F32
     )
 
-    for step in plane_steps(0, True):
+    def zrow_all(core):
+        region = w_proj.at[:, :, :, core, ring_rows, :]
+        return remote(region, region, zpair_s.at[0], zpair_r.at[0], partner)
+
+    wide_steps = plane_steps(0, True)
+    for i, step in enumerate(wide_steps):
+        if i == len(wide_steps) // 3:
+            for d in range(3, far):
+                zrow_step(d)
+        if i == len(wide_steps) * 2 // 3:
+            if far > 2:
+                zrow_step(far)
+            zrow_all(c).start()
         for order in range(2):
             d, dr, hf = step
             plane_wait(order, True, d, dr, hf)
@@ -379,6 +436,7 @@
         for order in range(2):
             wpair_wait(order, d, dr, hf, (order, hf, 1 + (d - 1) * 2 + dr))
 
+    zrow_all(1 - c).wait_recv()
     w_tiles = width // tile
 
     def project(i, carry):
@@ -668,6 +726,7 @@
         out[:, cut(ch)] = (mixed[:, cut(ch)].astype(F32) + expert_out).astype(BF)
     for t in range(1, n_tp):
         a2a_copy(t, lax.rem(me + t, n_tp)).wait_send()
+    zrow_all(c).wait_send()
     for copy in sends:
         copy.wait_send()
 
@@ -741,6 +800,7 @@
     buffers = [pltpu.VMEM(s, BF) if s is not None else pltpu.VMEM(next(f32_bufs), F32) for s in bf_bufs]
     sems = [(4,)]
     sems += [(2, 2)] * 2 + [(n_tp,)] * 2 + [(n_z,)] * 2 + [(2, 2, 2, 2)] * 4 + [(2, 2, 5)] * 2
+    sems += [(2, far, 2)] * 2 + [(1,)] * 2 + [(width // 256,)]
     sems += [(experts, 3)] + [(CHUNKS, n_sp)] * 2 + [(2, far, 2, CHUNKS)] * 2 + [(2, far, 2)] * 2 + [(n_z, 2)] * 4 + [(n_z,)] * 2
     sems += [(2, far + 1, 2, CHUNKS)] * 2 + [(CHUNKS, n_sp)] * 2
     return pl.pallas_call(

time: 180 us -> 174 us (0.967)
  Pallas kernels: 177 us -> 171 us
    pallas_call x1, Pallas kernels: 177 us -> 171 us  [per_device(): pl.pallas_call(functools.partial(layer_kernel, n_sp, n_x, n_z, kv_share,...]
where the time goes in v4:
time: 174 us; the launch traced here: 173 us
  Pallas kernels  171 us (98%)
  local copies, waits for them, and re-layouts  1.88 us (1%)
    pallas_call x1, Pallas kernels, per_device(): pl.pallas_call(functools.partial(layer_kernel, n_sp, n_x, n_z, kv_share,...  171 us

profile of v4, /device:TPU:8, one launch (start us, length us, event | category | flops | bytes accessed | tf_op | source)
XLA Modules:
  0.0 173.4 jit_solution(12666381467797398301)
XLA Ops:
  0.7 170.8 %shard_map.163 = bf16[128,2048]{1,0:T(8,128)(2,1)} custom-call(bf16[2048,128]{1,0:T(8,128)(2,1)} %queries.1, bf16[2048,512]{1,0:T(8,128)(2,1)} %key_heads.1, bf16[2048,512]{1,0:T(8,128)(2,1)} %value_heads.1, f32[1,1]{1,0:T(1,128)} %bitcast.6.sink, bf16[128,2048]{1,0:T(8,128)(2,1)} %out_weight.1, bf16[128,2048]{1,0:T(8,128)(2,1)} %residual.1, ...), custom_call_target="tpu_custom_call" | custom-call | tf_op jit(solution)/shard_map/pallas_call | solution.py:806
  171.5 1.9 %copy.20 = bf16[128,2048]{1,0:T(8,128)(2,1)} copy(bf16[128,2048]{1,0:T(8,128)(2,1)} %shard_map.163) | data formatting | bytes 1048576

commit v5 on v4

--- a/solution.py
+++ b/solution.py
@@ -445,7 +445,7 @@
         proj[:, columns] = jnp.dot(by_token[...], block, preferred_element_type=F32)
         return carry
 
-    lax.fori_loop(0, w_tiles, project, 0)
+    lax.fori_loop(0, w_tiles, project, 0, unroll=4)
 
     def norms(i, carry):
         at_rows = pl.ds(pl.multiple_of(i * 16, 16), 16)
@@ -458,7 +458,7 @@
         normed[at_rows, :] = (mixed_f * scale * expert_gain[...]).astype(BF)
         return carry
 
-    lax.fori_loop(0, tok // 16, norms, 0)
+    lax.fori_loop(0, tok // 16, norms, 0, unroll=4)
 
     head = jnp.dot(placing[...], normed[:, 0:128], preferred_element_type=F32)
     send[:, 0:128] = (head + gate_rows[...]).astype(BF)
@@ -577,7 +577,7 @@
                 oth[step, pl.ds(sub * hr, hr), columns] = piece[(sub * 2 + 1) * hr : (sub * 2 + 2) * hr]
             return carry
 
-        lax.fori_loop(0, width // tile, down, 0)
+        lax.fori_loop(0, width // tile, down, 0, unroll=2)
         summed[step] = push(oth.at[step], got.at[step], sum_s.at[step], sum_r.at[step], partner)
 
     hops = {}

time: 174 us -> 172 us (0.989)
  Pallas kernels: 171 us -> 168 us
    pallas_call x1, Pallas kernels: 171 us -> 168 us  [per_device(): pl.pallas_call(functools.partial(layer_kernel, n_sp, n_x, n_z, kv_share,...]
where the time goes in v5:
time: 172 us; the launch traced here: 170 us
  Pallas kernels  168 us (98%)
  local copies, waits for them, and re-layouts  1.88 us (1%)
    pallas_call x1, Pallas kernels, per_device(): pl.pallas_call(functools.partial(layer_kernel, n_sp, n_x, n_z, kv_share,...  168 us

profile of v5, /device:TPU:8, one launch (start us, length us, event | category | flops | bytes accessed | tf_op | source)
XLA Modules:
  0.0 170.3 jit_solution(292000309116908956)
XLA Ops:
  0.7 167.7 %shard_map.163 = bf16[128,2048]{1,0:T(8,128)(2,1)} custom-call(bf16[2048,128]{1,0:T(8,128)(2,1)} %queries.1, bf16[2048,512]{1,0:T(8,128)(2,1)} %key_heads.1, bf16[2048,512]{1,0:T(8,128)(2,1)} %value_heads.1, f32[1,1]{1,0:T(1,128)} %bitcast.6.sink, bf16[128,2048]{1,0:T(8,128)(2,1)} %out_weight.1, bf16[128,2048]{1,0:T(8,128)(2,1)} %residual.1, ...), custom_call_target="tpu_custom_call" | custom-call | tf_op jit(solution)/shard_map/pallas_call | solution.py:806
  168.4 1.9 %copy.20 = bf16[128,2048]{1,0:T(8,128)(2,1)} copy(bf16[128,2048]{1,0:T(8,128)(2,1)} %shard_map.163) | data formatting | bytes 1048576
